TPU v7x, 32 devices: a whole 2x2x4 slice. The times are simulated.
32 devices in a mesh: sp: 16 (over z, y, x), tp: 2 (over core).
Axes of the slice: x: 2, y: 2, z: 4, core: 2. Of those that a mesh axis runs over, the one named last changes fastest.
Arguments:
- residual_in: bfloat16 [6144, 2048], P(('sp', 'tp')), may hold values from -6 to 6
- conv_values: bfloat16 [6144, 1024], P('sp', 'tp'), may hold values from -60 to 60
- conv_gates: bfloat16 [6144, 1024], P('sp', 'tp'), may hold values from -8 to 8
- conv_kernel: float32 [31, 1024], P(None, 'tp'), may hold values from -1 to 1
- conv_bias: float32 [1024], P('tp'), may hold values from -3 to 3
- chan_gain: float32 [1024], P('tp'), may hold values from 0.1 to 1.9
- chan_shift: float32 [1024], P('tp'), may hold values from -3 to 3
- out_weight: bfloat16 [1024, 2048], replicated, may hold values from -0.1875 to 0.1875
- norm_gain: float32 [2048], replicated, may hold values from 0.1 to 1.9
- route_ids: int32 [6144, 2], P(('sp', 'tp')), may hold values from 0 to 15, all different within a row; in each aligned block of 192 rows (0 to 191, 192 to 383, ...) at most 48 rows name the same one
- route_weights: float32 [6144, 2], P(('sp', 'tp')), may hold values from 0.25 to 1.5
- expert_gate: bfloat16 [16, 2048, 2048], P('sp', None, 'tp'), may hold values from -0.125 to 0.125
- expert_up: bfloat16 [16, 2048, 2048], P('sp', None, 'tp'), may hold values from -0.125 to 0.125
- expert_down: bfloat16 [16, 2048, 2048], P('sp', 'tp'), may hold values from -0.125 to 0.125
Outputs:
- layer_out: bfloat16 [6144, 2048], P(('sp', 'tp'))
Inputs may be any that keep to these rules, and one draw needn't show every extreme that they name: `route_ids`: each row names 2 different experts. Among the rows of one device (aligned blocks of 192 rows) no expert is named by more than 48 rows, a bound that some block reaches.
All inputs are finite; a program needn't handle non-finite values.
Results may differ from a plain program's by a relative error of at most 0.014.
Values may be sent and summed in bfloat16 or wider, within the bound.
No kernel may reach another device: no remote copies, remote signals or barrier semaphores. Data moves between devices by JAX's collectives and lax.ppermute only.
A program may use at most 128 MiB of HBM per device.

v0:
```python
import jax
import jax.numpy as jnp
from jax import lax
from jax.sharding import PartitionSpec as P


def from_behind(value, axis, steps):
    count = lax.axis_size(axis)
    first, last = (max(0, -steps), min(count, count - steps))
    return lax.ppermute(value, axis, [(source, source + steps) for source in range(first, last)])


def on_device(
    residual_in,
    conv_values,
    conv_gates,
    conv_kernel,
    conv_bias,
    chan_gain,
    chan_shift,
    out_weight,
    norm_gain,
    route_ids,
    route_weights,
    expert_gate,
    expert_up,
    expert_down,
):
    taps_count = conv_kernel.shape[0]
    tok_count, local_chan = conv_values.shape
    tp_count = lax.axis_size("tp")
    all_chan = local_chan * tp_count
    gated = (
        conv_values.astype(jnp.float32) * jax.nn.sigmoid(conv_gates.astype(jnp.float32))
    ).astype(jnp.bfloat16)
    earlier = from_behind(gated[tok_count - (taps_count - 1) :], "sp", 1)
    extended = jnp.concatenate([earlier, gated], 0).astype(jnp.float32)
    mixed = jnp.zeros((tok_count, local_chan), jnp.float32) + conv_bias[None, :]
    for tap_index in range(taps_count):
        mixed = (
            mixed + conv_kernel[tap_index][None, :] * extended[tap_index : tap_index + tok_count]
        )
    row_total = jnp.sum(mixed, 1)
    row_square = jnp.sum(mixed * mixed, 1)
    row_total, row_square = lax.psum((row_total, row_square), "tp")
    center = (row_total / all_chan)[:, None]
    spread = (row_square / all_chan)[:, None] - center * center
    normed = (mixed - center) * lax.rsqrt(spread + 1e-06) * chan_gain[None, :] + chan_shift[None, :]
    activated = jax.nn.silu(normed).astype(jnp.bfloat16)
    row_count = tok_count // tp_count
    regrouped = lax.all_to_all(activated, "tp", split_axis=0, concat_axis=1, tiled=True)
    projected = jnp.dot(regrouped, out_weight, preferred_element_type=jnp.float32)
    after_f = (residual_in.astype(jnp.float32) + projected).astype(jnp.bfloat16).astype(jnp.float32)
    normal_rows = (
        after_f
        * lax.rsqrt(jnp.mean(after_f * after_f, 1, keepdims=True) + 1e-06)
        * norm_gain[None, :]
    ).astype(jnp.bfloat16)
    model_width = normal_rows.shape[1]
    experts_all = expert_gate.shape[0] * lax.axis_size("sp")
    choose_count = route_ids.shape[1]
    slot_cap = max(2, (2 * choose_count * row_count + experts_all - 1) // experts_all)
    onehot = (
        route_ids.reshape(-1)[:, None] == jnp.arange(experts_all, dtype=jnp.int32)[None, :]
    ).astype(jnp.int32)
    before = jnp.cumsum(onehot, 0) - onehot
    ranking = jnp.sum(before * onehot, 1).reshape(row_count, choose_count)
    slot_ids = route_ids * slot_cap + ranking
    positions = lax.broadcasted_iota(jnp.int32, (experts_all * slot_cap, 1, 1), 0)
    dispatch = jnp.any(positions == slot_ids[None, :, :], axis=2).astype(jnp.bfloat16)
    sendable = jnp.dot(dispatch, normal_rows, preferred_element_type=jnp.float32).astype(
        jnp.bfloat16
    )
    sendable = sendable.reshape(experts_all, slot_cap, model_width)
    both_rows = lax.all_gather(
        lax.all_to_all(sendable, "sp", split_axis=0, concat_axis=0, tiled=True),
        "tp",
        axis=0,
        tiled=True,
    )
    leading, slot_width, widths = both_rows.shape
    flat_rows = both_rows.reshape(leading * slot_width, widths)
    gate = jnp.dot(flat_rows, expert_gate[0], preferred_element_type=jnp.float32)
    upper = jnp.dot(flat_rows, expert_up[0], preferred_element_type=jnp.float32)
    hidden = (jax.nn.silu(gate) * upper).astype(jnp.bfloat16)
    summed = lax.psum_scatter(
        jnp.dot(hidden, expert_down[0], preferred_element_type=jnp.float32)
        .reshape(leading, slot_width, widths)
        .astype(jnp.bfloat16),
        "tp",
        scatter_dimension=0,
        tiled=True,
    )
    results = lax.all_to_all(summed, "sp", split_axis=0, concat_axis=0, tiled=True)
    flat_out = results.reshape(experts_all * slot_cap, model_width)
    picked = (
        jnp.take(flat_out, slot_ids.reshape(-1), axis=0)
        .reshape(row_count, choose_count, model_width)
        .astype(jnp.float32)
    )
    combined = after_f + jnp.sum(route_weights[:, :, None] * picked, 1)
    return combined.astype(jnp.bfloat16)


def solution(mesh):
    placed = (
        P(("sp", "tp"), None),
        P("sp", "tp"),
        P("sp", "tp"),
        P(None, "tp"),
        P("tp"),
        P("tp"),
        P("tp"),
        P(),
        P(),
        P(("sp", "tp"), None),
        P(("sp", "tp"), None),
        P("sp", None, "tp"),
        P("sp", None, "tp"),
        P("sp", "tp", None),
    )
    return jax.shard_map(
        on_device, mesh=mesh, in_specs=placed, out_specs=P(("sp", "tp"), None), check_vma=False
    )
```

profile of v0, /device:TPU:14, one launch (start us, length us, event | category | flops | bytes accessed | tf_op | source)
XLA Modules:
  0.0 266.2 jit_solution(6359469079230641675)
XLA Ops:
  6.5 1.3 multiply_convert_fusion.4
  7.9 3.4 %collective-permute-start = (bf16[30,512]{1,0:T(8,128)(2,1)S(1)}, bf16[30,512]{1,0:T(8,128)(2,1)S(1)}, u32[]{:S(2)}, u32[]{:S(2)}) collective-permute-start(bf16[30,512]{1,0:T(8,128)(2,1)S(1)} %slice.262), channel_id=1, source_target_pairs={{0,2},{2,4},{4,6},{6,8},{8,10},{10,12},{12,14},{14,16},{16,18},{18... | collective-permute-start | bytes 92168 | tf_op jit(solution)/shard_map/ppermute | solution.py:10
  11.3 1.2 fusion.47
  12.5 1.0 fusion.48
  13.5 0.8 copy.42
  14.6 0.9 reduce-window.6
  17.1 3.8 %fusion.45 = (f32[384]{0:T(512)S(1)}, f32[384]{0:T(512)S(1)}, f32[384,512]{1,0:T(8,128)S(1)}) fusion(f32[414,512]{1,0:T(8,128)S(1)} %maximum_convert_fusion, f32[512]{0:T(512)S(1)} %bitcast.110, f32[512]{0:T(512)S(1)} %bitcast.111, f32[512]{0:T(512)S(1)} %bitcast.82, f32[512]{0:T(512)S(1)} %bitcast.83, f32[512]{0:T(512)S(1)} %bitcast.84, ...), kind=kLoop, calls=%fused_computation.104 | loop fusion | flops 12778752 | bytes 25234432 | tf_op jit(solution)/shard_map/reduce_sum | solution.py:43
  20.9 2.6 all-reduce
  23.9 4.0 %all_to_all.29 = bf16[2,192,512]{2,1,0:T(8,128)(2,1)S(1)} all-to-all(bf16[2,192,512]{2,1,0:T(8,128)(2,1)S(1)} %bitcast.79), channel_id=1, replica_groups=mesh['sp'=16,'tp'=2] {'tp'}, dimensions={0} | all-to-all | bytes 786432 | tf_op jit(solution)/shard_map/all_to_all | solution.py:51
  28.0 3.3 %multiply_reduce_fusion.1 = (f32[192]{0:T(256)S(1)}, f32[192,2048]{1,0:T(8,128)S(1)}) fusion(bf16[192,1024]{1,0:T(8,128)(2,1)S(1)} %bitcast.77, bf16[1024,2048]{1,0:T(8,128)(2,1)} %param.21, bf16[192,2048]{1,0:T(8,128)(2,1)S(1)} %copy-done.2), kind=kOutput, calls=%fused_computation.15 | convolution fusion | flops 807665472 | bytes 6947584 | tf_op jit(solution)/shard_map/dot_general | solution.py:52
  31.4 1.2 copy-done
  32.6 1.1 convolution_convert_fusion.1
  33.7 75.6 %all_to_all.30 = bf16[16,48,2048]{2,1,0:T(8,128)(2,1)} all-to-all(bf16[16,48,2048]{2,1,0:T(8,128)(2,1)S(1)} %bitcast.76), channel_id=1, replica_groups=mesh['sp'=16,'tp'=2] {'sp'}, dimensions={0} | all-to-all | bytes 6291456 | tf_op jit(solution)/shard_map/all_to_all | solution.py:76
  109.5 16.9 %all-gather.2.cloned.1.call-done = bf16[32,48,2048]{2,1,0:T(8,128)(2,1)} async-done(((bf16[16,48,2048]{2,1,0:T(8,128)(2,1)}), bf16[32,48,2048]{2,1,0:T(8,128)(2,1)}) %all-gather.2.cloned.1.call-update) | async-done | bytes 6291472 | tf_op jit(solution)/shard_map/all_gather | solution.py:75
  126.4 10.1 %fusion.2 = f32[1536,1024]{1,0:T(8,128)S(1)} fusion(bf16[1536,2048]{1,0:T(8,128)(2,1)} %bitcast.112, bf16[1,2048,1024]{2,1,0:T(8,128)(2,1)} %param.25), kind=kOutput, calls=%fused_computation.5 | convolution fusion | flops 6442450944 | bytes 16777216 | tf_op jit(solution)/shard_map/dot_general | solution.py:83
  136.6 7.4 %multiply_convert_fusion = bf16[1536,1024]{1,0:T(8,128)(2,1)S(1)} fusion(f32[1536,1024]{1,0:T(8,128)S(1)} %fusion.2, bf16[1536,2048]{1,0:T(8,128)(2,1)S(1)} %bitcast.113, bf16[1,2048,1024]{2,1,0:T(8,128)(2,1)S(1)} %copy-done.9), kind=kOutput, calls=%fused_computation.1 | convolution fusion | flops 6451888128 | bytes 19922944 | tf_op jit(solution)/shard_map/dot_general | solution.py:84
  144.1 8.8 %convolution_convert_fusion = bf16[32,48,2048]{2,1,0:T(8,128)(2,1)} fusion(bf16[32,48,1024]{2,1,0:T(8,128)(2,1)S(1)} %bitcast.114, bf16[1,1024,2048]{2,1,0:T(8,128)(2,1)S(1)} %copy-done.10), kind=kOutput, calls=%fused_computation.2 | convolution fusion | flops 6445596672 | bytes 13631488 | tf_op jit(solution)/shard_map/dot_general | solution.py:87
  152.9 16.2 %reduce-scatter.2.cloned.1.call-done = bf16[16,48,2048]{2,1,0:T(8,128)(2,1)} async-done(((bf16[32,48,2048]{2,1,0:T(8,128)(2,1)}), bf16[16,48,2048]{2,1,0:T(8,128)(2,1)}) %reduce-scatter.2.cloned.1.call-update) | async-done | bytes 3145744 | tf_op jit(solution)/shard_map/reduce_scatter | solution.py:86
  169.1 7.0 %all-to-all-start.2 = ((bf16[16,48,2048]{2,1,0:T(8,128)(2,1)}), bf16[16,48,2048]{2,1,0:T(8,128)(2,1)S(1)}, u32[]{:S(2)}, u32[]{:S(2)}) async-start(bf16[16,48,2048]{2,1,0:T(8,128)(2,1)} %reduce-scatter.2.cloned.1.call-done), calls=%async_computation.3 | async-start | bytes 6291456 | tf_op jit(solution)/shard_map/all_to_all | solution.py:94
  176.6 69.5 %all-to-all-done.2 = bf16[16,48,2048]{2,1,0:T(8,128)(2,1)S(1)} async-done(((bf16[16,48,2048]{2,1,0:T(8,128)(2,1)}), bf16[16,48,2048]{2,1,0:T(8,128)(2,1)S(1)}, u32[]{:S(2)}, u32[]{:S(2)}) %all-to-all-start.2) | async-done | bytes 3145760 | tf_op jit(solution)/shard_map/all_to_all | solution.py:94
  246.1 3.1 %gather_fusion = bf16[384,2048]{1,0:T(8,128)(2,1)} fusion(bf16[768,2048]{1,0:T(8,128)(2,1)S(1)} %bitcast.75, s32[1024]{0:T(1024)S(1)} %pad_clamp_fusion), kind=kCustom, calls=%fused_computation | custom fusion | bytes 3147264 | tf_op jit(solution)/shard_map/jit(_take)/gather | solution.py:97
  249.2 2.9 %gather.7 = bf16[192,2,2048]{2,1,0:T(2,128)(2,1)S(1)} reshape(bf16[384,2048]{1,0:T(8,128)(2,1)} %gather_fusion) | data formatting | bytes 3145728 | tf_op jit(solution)/shard_map/jit(_take)/gather | solution.py:97
  252.1 6.1 %multiply_reduce_fusion = f32[192,2048]{1,0:T(8,128)S(1)} fusion(bf16[192,2,2048]{2,1,0:T(2,128)(2,1)S(1)} %gather.7, pred[192,2]{1,0:T(8,128)(4,1)S(1)} %copy.46, f32[192,2]{1,0:T(8,128)S(1)} %copy.41), kind=kLoop, calls=%fused_computation.8 | loop fusion | flops 2752512 | bytes 3147648 | tf_op jit(solution)/shard_map/reduce_sum | solution.py:101
  258.3 1.1 add_convert_fusion
  (48 shorter events, 3.1 us)
Async XLA Ops:
  6.5 10.5 %copy-start.7 = (f32[512]{0:T(512)S(1)}, f32[512]{0:T(512)}, u32[]{:S(2)}) copy-start(f32[512]{0:T(512)} %param.18) | copy-start | bytes 6148
  6.5 119.9 %all-gather.2.cloned.1.call-start = ((), (), s32[]{:S(2)}) async-start(), calls=%async_computation.4 | async-start | bytes 9437184 | tf_op jit(solution)/shard_map/all_gather | solution.py:75
  7.9 9.0 %collective-permute-start = (bf16[30,512]{1,0:T(8,128)(2,1)S(1)}, bf16[30,512]{1,0:T(8,128)(2,1)S(1)}, u32[]{:S(2)}, u32[]{:S(2)}) collective-permute-start(bf16[30,512]{1,0:T(8,128)(2,1)S(1)} %slice.262), channel_id=1, source_target_pairs={{0,2},{2,4},{4,6},{6,8},{8,10},{10,12},{12,14},{14,16},{16,18},{18... | collective-permute-start | bytes 92168 | tf_op jit(solution)/shard_map/ppermute | solution.py:10
  17.1 6.5 %copy-start.4 = (f32[512]{0:T(512)S(1)}, f32[512]{0:T(512)}, u32[]{:S(2)}) copy-start(f32[512]{0:T(512)} %param.20) | copy-start | bytes 6148
  17.1 6.5 %copy-start.5 = (f32[512]{0:T(512)S(1)}, f32[512]{0:T(512)}, u32[]{:S(2)}) copy-start(f32[512]{0:T(512)} %param.19) | copy-start | bytes 6148
  20.9 7.1 %copy-start.2 = (bf16[192,2048]{1,0:T(8,128)(2,1)S(1)}, bf16[192,2048]{1,0:T(8,128)(2,1)}, u32[]{:S(2)}) copy-start(bf16[192,2048]{1,0:T(8,128)(2,1)} %param.14) | copy-start | bytes 2359300
  28.0 4.5 %copy-start.3 = (f32[2048]{0:T(1024)S(1)}, f32[2048]{0:T(1024)}, u32[]{:S(2)}) copy-start(f32[2048]{0:T(1024)} %param.22) | copy-start | bytes 24580
  31.4 1.2 copy-start
  109.3 59.8 %reduce-scatter.2.cloned.1.call-start = ((), (), s32[]{:S(2)}) async-start(), calls=%async_computation.5 | async-start | bytes 9437184 | tf_op jit(solution)/shard_map/reduce_scatter | solution.py:86
  126.4 10.1 %copy-start.8 = (bf16[32,48,2048]{2,1,0:T(8,128)(2,1)S(1)}, bf16[32,48,2048]{2,1,0:T(8,128)(2,1)}, u32[]{:S(2)}) copy-start(bf16[32,48,2048]{2,1,0:T(8,128)(2,1)} %all-gather.2.cloned.1.call-done) | copy-start | bytes 18874372
  126.4 10.1 %copy-start.9 = (bf16[1,2048,1024]{2,1,0:T(8,128)(2,1)S(1)}, bf16[1,2048,1024]{2,1,0:T(8,128)(2,1)}, u32[]{:S(2)}) copy-start(bf16[1,2048,1024]{2,1,0:T(8,128)(2,1)} %param.26) | copy-start | bytes 12582916
  136.6 7.5 %copy-start.10 = (bf16[1,1024,2048]{2,1,0:T(8,128)(2,1)S(1)}, bf16[1,1024,2048]{2,1,0:T(8,128)(2,1)}, u32[]{:S(2)}) copy-start(bf16[1,1024,2048]{2,1,0:T(8,128)(2,1)} %param.27) | copy-start | bytes 12582916
  152.9 23.6 %copy-start.6 = (f32[192,2]{0,1:T(2,128)S(1)}, f32[192,2]{0,1:T(2,128)}, u32[]{:S(2)}) copy-start(f32[192,2]{0,1:T(2,128)} %param.24) | copy-start | bytes 4612
  169.1 77.0 %all-to-all-start.2 = ((bf16[16,48,2048]{2,1,0:T(8,128)(2,1)}), bf16[16,48,2048]{2,1,0:T(8,128)(2,1)S(1)}, u32[]{:S(2)}, u32[]{:S(2)}) async-start(bf16[16,48,2048]{2,1,0:T(8,128)(2,1)} %reduce-scatter.2.cloned.1.call-done), calls=%async_computation.3 | async-start | bytes 6291456 | tf_op jit(solution)/shard_map/all_to_all | solution.py:94
  249.2 9.0 %copy-start.1 = (f32[192,2048]{1,0:T(8,128)S(1)}, f32[192,2048]{1,0:T(8,128)}, u32[]{:S(2)}) copy-start(f32[192,2048]{1,0:T(8,128)} %copy-done) | copy-start | bytes 4718596
Sparse Core Ops, SparseCore 0:
  109.4 16.9 all-gather.1
  153.0 16.0 reduce-scatter.1
where the time goes:
time: 267 us; the launch traced here: 266 us
  waiting for transfers between devices  103 us (39%)
  blocking collectives  82.3 us (31%)
  matrix products  30.7 us (11%)
  other arithmetic  14.8 us (6%)
  between operations  13.7 us (5%)
  local copies, waits for them, and re-layouts  11.5 us (4%)
  starting transfers between devices  10.6 us (4%)
    all_to_all x1, blocking collectives, on_device(): lax.all_to_all(sendable, 'sp', split_axis=0, concat_axis=0, tiled=True)  75.6 us
    all_to_all x1, waiting for transfers between devices, on_device(): lax.all_to_all(summed, 'sp', split_axis=0, concat_axis=0, tiled=True)  69.5 us
    all_gather x1, waiting for transfers between devices, on_device(): lax.all_gather(lax.all_to_all(sendable, 'sp', split_axis=0, concat_axis=0...  16.9 us
    reduce_scatter x1, waiting for transfers between devices, on_device(): lax.psum_scatter(jnp.dot(hidden, expert_down[0], preferred_element_type=j...  16.2 us
    dot_general x1, matrix products, on_device(): jnp.dot(flat_rows, expert_gate[0], preferred_element_type=jnp.float32)  10.1 us
    dot_general x1, matrix products, on_device(): jnp.dot(hidden, expert_down[0], preferred_element_type=jnp.float32)  8.76 us
    dot_general x1, matrix products, on_device(): upper = jnp.dot(flat_rows, expert_up[0], preferred_element_type=jnp.float32)  7.44 us
    all_to_all x1, starting transfers between devices, on_device(): lax.all_to_all(summed, 'sp', split_axis=0, concat_axis=0, tiled=True)  6.96 us
  transfers between devices with their start and end apart: 4, of which 3 were waited for; matrix products, arithmetic and copies ran while one was open for 2% of the time, Pallas kernels for 0%

commit v1 on v0

--- a/solution.py
+++ b/solution.py
@@ -72,33 +72,31 @@
         jnp.bfloat16
     )
     sendable = sendable.reshape(experts_all, slot_cap, model_width)
-    both_rows = lax.all_gather(
-        lax.all_to_all(sendable, "sp", split_axis=0, concat_axis=0, tiled=True),
-        "tp",
-        axis=0,
-        tiled=True,
-    )
-    leading, slot_width, widths = both_rows.shape
-    flat_rows = both_rows.reshape(leading * slot_width, widths)
-    gate = jnp.dot(flat_rows, expert_gate[0], preferred_element_type=jnp.float32)
-    upper = jnp.dot(flat_rows, expert_up[0], preferred_element_type=jnp.float32)
-    hidden = (jax.nn.silu(gate) * upper).astype(jnp.bfloat16)
-    summed = lax.psum_scatter(
-        jnp.dot(hidden, expert_down[0], preferred_element_type=jnp.float32)
-        .reshape(leading, slot_width, widths)
-        .astype(jnp.bfloat16),
-        "tp",
-        scatter_dimension=0,
-        tiled=True,
-    )
+    received = lax.all_to_all(sendable, "sp", split_axis=0, concat_axis=0, tiled=True)
+    flat_rows = received.reshape(experts_all * slot_cap, model_width)
+    halves = [(expert_gate[0], expert_up[0], expert_down[0])]
+    for shift in range(1, tp_count):
+        turn = [(source, (source + shift) % tp_count) for source in range(tp_count)]
+        halves.append(
+            tuple(
+                lax.ppermute(held[0], "tp", turn) for held in (expert_gate, expert_up, expert_down)
+            )
+        )
+    total = 0.0
+    for gate_w, up_w, down_w in halves:
+        gate = jnp.dot(flat_rows, gate_w, preferred_element_type=jnp.float32)
+        upper = jnp.dot(flat_rows, up_w, preferred_element_type=jnp.float32)
+        hidden = (jax.nn.silu(gate) * upper).astype(jnp.bfloat16)
+        total = total + jnp.dot(hidden, down_w, preferred_element_type=jnp.float32)
+    summed = total.astype(jnp.bfloat16).reshape(experts_all, slot_cap, model_width)
     results = lax.all_to_all(summed, "sp", split_axis=0, concat_axis=0, tiled=True)
     flat_out = results.reshape(experts_all * slot_cap, model_width)
-    picked = (
-        jnp.take(flat_out, slot_ids.reshape(-1), axis=0)
-        .reshape(row_count, choose_count, model_width)
-        .astype(jnp.float32)
-    )
-    combined = after_f + jnp.sum(route_weights[:, :, None] * picked, 1)
+    slots = lax.broadcasted_iota(jnp.int32, (1, experts_all * slot_cap), 1)
+    combined = after_f
+    for choice in range(choose_count):
+        chosen = (slots == slot_ids[:, choice : choice + 1]).astype(jnp.bfloat16)
+        picked = jnp.dot(chosen, flat_out, preferred_element_type=jnp.float32)
+        combined = combined + route_weights[:, choice : choice + 1] * picked
     return combined.astype(jnp.bfloat16)
 
 

time: 267 us -> 228 us (0.85)
  blocking collectives: 82.3 us -> 6.65 us
  waiting for transfers between devices: 103 us -> 141 us
  matrix products: 30.7 us -> 51.8 us
  between operations: 13.7 us -> 0.22 us
  other arithmetic: 14.8 us -> 7.54 us
  local copies, waits for them, and re-layouts: 11.5 us -> 4.94 us
  starting transfers between devices: 10.6 us -> 15.5 us
    all_to_all x1 -> x0, blocking collectives: 75.6 us -> none  [on_device(): lax.all_to_all(sendable, 'sp', split_axis=0, concat_axis=0, tiled=True)]
    all_to_all x0 -> x1, waiting for transfers between devices: none -> 71.1 us  [on_device(): lax.all_to_all(sendable, 'sp', split_axis=0, concat_axis=0, tiled=True)]
    dot_general x3 -> x6, matrix products: 26.3 us -> 45.8 us  [the longest x2 27.2 us: on_device(): total = total + jnp.dot(hidden, down_w, preferred_element_type=jnp.float32)]
    all_gather x1 -> x0, waiting for transfers between devices: 16.9 us -> none  [on_device(): lax.all_gather(lax.all_to_all(sendable, 'sp', split_axis=0, concat_axis=0...]
    reduce_scatter x1 -> x0, waiting for transfers between devices: 16.2 us -> none  [on_device(): lax.psum_scatter(jnp.dot(hidden, expert_down[0], preferred_element_type=j...]
    all_to_all x0 -> x1, starting transfers between devices: none -> 6.21 us  [on_device(): lax.all_to_all(sendable, 'sp', split_axis=0, concat_axis=0, tiled=True)]
    reduce_sum x1 -> x0, other arithmetic: 6.11 us -> none  [on_device(): combined = after_f + jnp.sum(route_weights[:, :, None] * picked, 1)]
    gather x2 -> x0, local copies, waits for them, and re-layouts: 6.02 us -> none  [on_device(): jnp.take(flat_out, slot_ids.reshape(-1), axis=0)]
  transfers between devices with their start and end apart: 4 -> 6, of which waited for: 3 -> 2; matrix products, arithmetic and copies ran while one was open for 2% -> 15% of each run, Pallas kernels for 0% -> 0%
where the time goes in v1:
time: 228 us; the launch traced here: 227 us
  waiting for transfers between devices  141 us (62%)
  matrix products  51.8 us (23%)
  starting transfers between devices  15.5 us (7%)
  other arithmetic  7.54 us (3%)
  blocking collectives  6.65 us (3%)
  local copies, waits for them, and re-layouts  4.94 us (2%)
    all_to_all x1, waiting for transfers between devices, on_device(): lax.all_to_all(sendable, 'sp', split_axis=0, concat_axis=0, tiled=True)  71.1 us
    all_to_all x1, waiting for transfers between devices, on_device(): lax.all_to_all(summed, 'sp', split_axis=0, concat_axis=0, tiled=True)  69.7 us
    dot_general x2, matrix products, on_device(): total = total + jnp.dot(hidden, down_w, preferred_element_type=jnp.float32)  27.2 us
    dot_general x2, matrix products, on_device(): gate = jnp.dot(flat_rows, gate_w, preferred_element_type=jnp.float32)  14.5 us
    all_to_all x1, starting transfers between devices, on_device(): lax.all_to_all(sendable, 'sp', split_axis=0, concat_axis=0, tiled=True)  6.21 us
    all_to_all x1, starting transfers between devices, on_device(): lax.all_to_all(summed, 'sp', split_axis=0, concat_axis=0, tiled=True)  5.25 us
  transfers between devices with their start and end apart: 6, of which 2 were waited for; matrix products, arithmetic and copies ran while one was open for 15% of the time, Pallas kernels for 0%

profile of v1, /device:TPU:14, one launch (start us, length us, event | category | flops | bytes accessed | tf_op | source)
XLA Modules:
  0.0 227.4 jit_solution(3078782395500073562)
XLA Ops:
  0.0 1.4 multiply_convert_fusion.6
  1.4 3.4 %collective-permute-start = (bf16[30,512]{1,0:T(8,128)(2,1)S(1)}, bf16[30,512]{1,0:T(8,128)(2,1)S(1)}, u32[]{:S(2)}, u32[]{:S(2)}) collective-permute-start(bf16[30,512]{1,0:T(8,128)(2,1)S(1)} %slice.276), channel_id=1, source_target_pairs={{0,2},{2,4},{4,6},{6,8},{8,10},{10,12},{12,14},{14,16},{16,18},{18... | collective-permute-start | bytes 92168 | tf_op jit(solution)/shard_map/ppermute | solution.py:10
  4.8 1.2 fusion.56
  6.0 1.0 fusion.57
  7.0 0.8 copy.42
  8.1 0.9 reduce-window.6
  9.5 0.7 multiply_add_fusion
  10.6 3.8 %fusion.54 = (f32[384]{0:T(512)S(1)}, f32[384]{0:T(512)S(1)}, f32[384,512]{1,0:T(8,128)S(1)}) fusion(f32[414,512]{1,0:T(8,128)S(1)} %maximum_convert_fusion, f32[512]{0:T(512)S(1)} %bitcast.127, f32[512]{0:T(512)S(1)} %bitcast.128, f32[512]{0:T(512)S(1)} %bitcast.99, f32[512]{0:T(512)S(1)} %bitcast.100, f32[512]{0:T(512)S(1)} %bitcast.101, ...), kind=kLoop, calls=%fused_computation.109 | loop fusion | flops 12778752 | bytes 25234432 | tf_op jit(solution)/shard_map/reduce_sum | solution.py:43
  14.4 2.6 %all-reduce = (f32[384]{0:T(512)S(1)}, f32[384]{0:T(512)S(1)}) all-reduce(f32[384]{0:T(512)S(1)} %get-tuple-element.6, f32[384]{0:T(512)S(1)} %get-tuple-element.5), channel_id=1, replica_groups=mesh['sp'=16,'tp'=2] {'tp'}, use_global_device_ids=true, to_apply=%region_3.0 | all-reduce | flops 768 | bytes 6144 | tf_op jit(solution)/shard_map/psum | solution.py:45
  17.4 4.0 %all_to_all.29 = bf16[2,192,512]{2,1,0:T(8,128)(2,1)S(1)} all-to-all(bf16[2,192,512]{2,1,0:T(8,128)(2,1)S(1)} %bitcast.94), channel_id=1, replica_groups=mesh['sp'=16,'tp'=2] {'tp'}, dimensions={0} | all-to-all | bytes 786432 | tf_op jit(solution)/shard_map/all_to_all | solution.py:51
  21.5 3.3 %multiply_reduce_fusion = (f32[192]{0:T(256)S(1)}, f32[192,2048]{1,0:T(8,128)S(1)}) fusion(bf16[192,1024]{1,0:T(8,128)(2,1)S(1)} %bitcast.92, bf16[1024,2048]{1,0:T(8,128)(2,1)} %param.21, bf16[192,2048]{1,0:T(8,128)(2,1)S(1)} %copy-done.1), kind=kOutput, calls=%fused_computation.14 | convolution fusion | flops 807665472 | bytes 6947584 | tf_op jit(solution)/shard_map/dot_general | solution.py:52
  24.9 1.2 copy-done
  26.0 2.7 %convolution_convert_fusion = bf16[768,2048]{1,0:T(8,128)(2,1)} fusion(pred[768,192]{0,1:T(8,128)(4,1)S(1)} %fusion.6, f32[192,2048]{1,0:T(8,128)S(1)} %get-tuple-element.48, f32[2048]{0:T(1024)S(1)} %copy-done.2, f32[192]{0:T(256)S(1)} %add_rsqrt_fusion.1), kind=kOutput, calls=%fused_computation.1 | convolution fusion | flops 606732288 | bytes 4875008 | tf_op jit(solution)/shard_map/dot_general | solution.py:71
  28.8 6.2 %all-to-all-start.1 = ((bf16[16,48,2048]{2,1,0:T(8,128)(2,1)}), bf16[16,48,2048]{2,1,0:T(8,128)(2,1)S(1)}, u32[]{:S(2)}, u32[]{:S(2)}) async-start(bf16[16,48,2048]{2,1,0:T(8,128)(2,1)} %bitcast.36), calls=%async_computation.1 | async-start | bytes 6291456 | tf_op jit(solution)/shard_map/all_to_all | solution.py:75
  35.1 0.5 collective-permute-start.2
  35.6 71.1 %all-to-all-done.1 = bf16[16,48,2048]{2,1,0:T(8,128)(2,1)S(1)} async-done(((bf16[16,48,2048]{2,1,0:T(8,128)(2,1)}), bf16[16,48,2048]{2,1,0:T(8,128)(2,1)S(1)}, u32[]{:S(2)}, u32[]{:S(2)}) %all-to-all-start.1) | async-done | bytes 3145760 | tf_op jit(solution)/shard_map/all_to_all | solution.py:75
  106.7 7.2 %fusion.50 = f32[768,1024]{1,0:T(8,128)} fusion(bf16[768,2048]{1,0:T(8,128)(2,1)S(1)} %bitcast.87, bf16[1,2048,1024]{2,1,0:T(8,128)(2,1)} %param.25), kind=kOutput, calls=%fused_computation.105 | convolution fusion | flops 3221225472 | bytes 10485760 | tf_op jit(solution)/shard_map/dot_general | solution.py:87
  113.9 7.2 %fusion.62 = f32[768,1024]{1,0:T(8,128)} fusion(bf16[768,2048]{1,0:T(8,128)(2,1)S(1)} %bitcast.88, bf16[2048,1024]{1,0:T(8,128)(2,1)} %collective-permute-done.1), kind=kOutput, calls=%fused_computation.115 | convolution fusion | flops 3221225472 | bytes 10485760 | tf_op jit(solution)/shard_map/dot_general | solution.py:87
  121.2 13.8 %fusion.40 = f32[768,2048]{1,0:T(8,128)} fusion(f32[768,1024]{1,0:T(8,128)} %fusion.50, bf16[768,2048]{1,0:T(8,128)(2,1)S(1)} %bitcast.89, bf16[1,1024,2048]{2,1,0:T(8,128)(2,1)} %param.27, bf16[1,2048,1024]{2,1,0:T(8,128)(2,1)} %param.26), kind=kOutput, calls=%fused_computation.84 | convolution fusion | flops 6447169536 | bytes 20971520 | tf_op jit(solution)/shard_map/dot_general | solution.py:90
  135.0 13.3 %add_convert_fusion = bf16[768,2048]{1,0:T(8,128)(2,1)} fusion(f32[768,2048]{1,0:T(8,128)} %fusion.40, bf16[1024,2048]{1,0:T(8,128)(2,1)} %collective-permute-done.3, f32[768,1024]{1,0:T(8,128)} %fusion.62, bf16[768,2048]{1,0:T(8,128)(2,1)S(1)} %bitcast.90, bf16[2048,1024]{1,0:T(8,128)(2,1)} %collective-permute-done.2), kind=kOutput, calls=%fused_computation | convolution fusion | flops 6450315264 | bytes 24117248 | tf_op jit(solution)/shard_map/dot_general | solution.py:90
  148.3 5.2 %all-to-all-start.2 = ((bf16[16,48,2048]{2,1,0:T(8,128)(2,1)}), bf16[16,48,2048]{2,1,0:T(8,128)(2,1)S(1)}, u32[]{:S(2)}, u32[]{:S(2)}) async-start(bf16[16,48,2048]{2,1,0:T(8,128)(2,1)} %bitcast.91), calls=%async_computation.2 | async-start | bytes 6291456 | tf_op jit(solution)/shard_map/all_to_all | solution.py:92
  153.6 69.7 %all-to-all-done.2 = bf16[16,48,2048]{2,1,0:T(8,128)(2,1)S(1)} async-done(((bf16[16,48,2048]{2,1,0:T(8,128)(2,1)}), bf16[16,48,2048]{2,1,0:T(8,128)(2,1)S(1)}, u32[]{:S(2)}, u32[]{:S(2)}) %all-to-all-start.2) | async-done | bytes 3145760 | tf_op jit(solution)/shard_map/all_to_all | solution.py:92
  223.3 2.3 %fusion.1 = f32[192,2048]{1,0:T(8,128)S(1)} fusion(f32[192,2048]{1,0:T(8,128)} %copy-done, bf16[768,2048]{1,0:T(8,128)(2,1)S(1)} %bitcast.85, f32[192]{0:T(256)S(1)} %bitcast.130, s32[192]{0:T(256)S(1)} %bitcast.129), kind=kOutput, calls=%fused_computation.7 | convolution fusion | flops 604913664 | bytes 6292992 | tf_op jit(solution)/shard_map/dot_general | solution.py:98
  225.6 1.8 fusion.4
  (36 shorter events, 1.8 us)
Async XLA Ops:
  0.0 10.5 %copy-start.6 = (f32[512]{0:T(512)S(1)}, f32[512]{0:T(512)}, u32[]{:S(2)}) copy-start(f32[512]{0:T(512)} %param.18) | copy-start | bytes 6148
  1.4 9.0 %collective-permute-start = (bf16[30,512]{1,0:T(8,128)(2,1)S(1)}, bf16[30,512]{1,0:T(8,128)(2,1)S(1)}, u32[]{:S(2)}, u32[]{:S(2)}) collective-permute-start(bf16[30,512]{1,0:T(8,128)(2,1)S(1)} %slice.276), channel_id=1, source_target_pairs={{0,2},{2,4},{4,6},{6,8},{8,10},{10,12},{12,14},{14,16},{16,18},{18... | collective-permute-start | bytes 92168 | tf_op jit(solution)/shard_map/ppermute | solution.py:10
  10.5 6.5 %copy-start.3 = (f32[512]{0:T(512)S(1)}, f32[512]{0:T(512)}, u32[]{:S(2)}) copy-start(f32[512]{0:T(512)} %param.20) | copy-start | bytes 6148
  10.6 6.5 %copy-start.4 = (f32[512]{0:T(512)S(1)}, f32[512]{0:T(512)}, u32[]{:S(2)}) copy-start(f32[512]{0:T(512)} %param.19) | copy-start | bytes 6148
  14.4 7.1 %copy-start.1 = (bf16[192,2048]{1,0:T(8,128)(2,1)S(1)}, bf16[192,2048]{1,0:T(8,128)(2,1)}, u32[]{:S(2)}) copy-start(bf16[192,2048]{1,0:T(8,128)(2,1)} %param.14) | copy-start | bytes 2359300
  21.5 4.5 %copy-start.2 = (f32[2048]{0:T(1024)S(1)}, f32[2048]{0:T(1024)}, u32[]{:S(2)}) copy-start(f32[2048]{0:T(1024)} %param.22) | copy-start | bytes 24580
  24.9 1.2 copy-start
  28.8 77.9 %all-to-all-start.1 = ((bf16[16,48,2048]{2,1,0:T(8,128)(2,1)}), bf16[16,48,2048]{2,1,0:T(8,128)(2,1)S(1)}, u32[]{:S(2)}, u32[]{:S(2)}) async-start(bf16[16,48,2048]{2,1,0:T(8,128)(2,1)} %bitcast.36), calls=%async_computation.1 | async-start | bytes 6291456 | tf_op jit(solution)/shard_map/all_to_all | solution.py:75
  35.0 79.0 %collective-permute-start.1 = (bf16[2048,1024]{1,0:T(8,128)(2,1)}, bf16[2048,1024]{1,0:T(8,128)(2,1)}, u32[]{:S(2)}, u32[]{:S(2)}) collective-permute-start(bf16[2048,1024]{1,0:T(8,128)(2,1)} %bitcast.131), channel_id=1, source_target_pairs={{0,1},{1,0},{2,3},{3,2},{4,5},{5,4},{6,7},{7,6},{8,9},{9,8},{10,11... | collective-permute-start | bytes 12582920 | tf_op jit(solution)/shard_map/ppermute | solution.py:82
  35.1 100.0 %collective-permute-start.2 = (bf16[2048,1024]{1,0:T(8,128)(2,1)}, bf16[2048,1024]{1,0:T(8,128)(2,1)}, u32[]{:S(2)}, u32[]{:S(2)}) collective-permute-start(bf16[2048,1024]{1,0:T(8,128)(2,1)} %bitcast.132), channel_id=1, source_target_pairs={{0,1},{1,0},{2,3},{3,2},{4,5},{5,4},{6,7},{7,6},{8,9},{9,8},{10,11... | collective-permute-start | bytes 12582920 | tf_op jit(solution)/shard_map/ppermute | solution.py:82
  35.6 99.5 %collective-permute-start.3 = (bf16[1024,2048]{1,0:T(8,128)(2,1)}, bf16[1024,2048]{1,0:T(8,128)(2,1)}, u32[]{:S(2)}, u32[]{:S(2)}) collective-permute-start(bf16[1024,2048]{1,0:T(8,128)(2,1)} %bitcast.133), channel_id=1, source_target_pairs={{0,1},{1,0},{2,3},{3,2},{4,5},{5,4},{6,7},{7,6},{8,9},{9,8},{10,11... | collective-permute-start | bytes 12582920 | tf_op jit(solution)/shard_map/ppermute | solution.py:82
  148.3 5.3 %copy-start.5 = (f32[192,2]{0,1:T(2,128)S(1)}, f32[192,2]{0,1:T(2,128)}, u32[]{:S(2)}) copy-start(f32[192,2]{0,1:T(2,128)} %param.24) | copy-start | bytes 4612
  148.3 74.9 %all-to-all-start.2 = ((bf16[16,48,2048]{2,1,0:T(8,128)(2,1)}), bf16[16,48,2048]{2,1,0:T(8,128)(2,1)S(1)}, u32[]{:S(2)}, u32[]{:S(2)}) async-start(bf16[16,48,2048]{2,1,0:T(8,128)(2,1)} %bitcast.91), calls=%async_computation.2 | async-start | bytes 6291456 | tf_op jit(solution)/shard_map/all_to_all | solution.py:92

commit v2 on v1

v2 whole, which is shorter than its diff:
```python
import functools

import jax
import jax.numpy as jnp
from jax import lax
from jax.experimental import pallas as pl
from jax.experimental.pallas import tpu as pltpu
from jax.sharding import PartitionSpec as P


def expert_body(count, own_steps, rows, *refs):
    gates, uppers, downs = (refs[:count], refs[count : 2 * count], refs[2 * count : 3 * count])
    out, hidden = refs[3 * count :]
    step = pl.program_id(0)
    width = gates[0].shape[1]
    for part in range(count):

        @pl.when((step >= part * own_steps) & (step < (part + 1) * own_steps))
        def _(part=part):
            gate = jnp.dot(rows[...], gates[part][...], preferred_element_type=jnp.float32)
            upper = jnp.dot(rows[...], uppers[part][...], preferred_element_type=jnp.float32)
            value = (gate * jax.nn.sigmoid(gate) * upper).astype(jnp.bfloat16)
            hidden[step] = value

    @pl.when(step >= count * own_steps)
    def _():
        total = None
        for part in range(count):
            for piece in range(own_steps):
                product = jnp.dot(
                    hidden[part * own_steps + piece],
                    downs[part][piece * width : (piece + 1) * width, :],
                    preferred_element_type=jnp.float32,
                )
                total = product if total is None else total + product
        out[...] = total.astype(jnp.bfloat16)


def expert_call(rows, gates, uppers, downs):
    count = len(gates)
    row_total, model_width = rows.shape
    own_hidden = gates[0].shape[1]
    width = min(512, own_hidden)
    own_steps = own_hidden // width
    first_steps = count * own_steps
    out_steps = model_width // width

    def inward(part):
        return pl.BlockSpec(
            (model_width, width),
            lambda i: (0, jnp.clip(i - part * own_steps, 0, own_steps - 1)),
        )

    outward = pl.BlockSpec(
        (own_hidden, width), lambda i: (0, jnp.clip(i - first_steps, 0, out_steps - 1))
    )
    return pl.pallas_call(
        functools.partial(expert_body, count, own_steps),
        grid=(first_steps + out_steps,),
        in_specs=[pl.BlockSpec((row_total, model_width), lambda i: (0, 0))]
        + [inward(part) for part in range(count)] * 2
        + [outward] * count,
        out_specs=pl.BlockSpec(
            (row_total, width), lambda i: (0, jnp.clip(i - first_steps, 0, out_steps - 1))
        ),
        out_shape=jax.ShapeDtypeStruct((row_total, model_width), jnp.bfloat16),
        scratch_shapes=[pltpu.VMEM((first_steps, row_total, width), jnp.bfloat16)],
        compiler_params=pltpu.CompilerParams(dimension_semantics=("arbitrary",)),
        cost_estimate=pl.CostEstimate(
            flops=6 * row_total * model_width * own_hidden * count,
            bytes_accessed=6 * model_width * own_hidden * count,
            transcendentals=row_total * own_hidden * count,
        ),
        name="expert_rows",
    )(rows, *gates, *uppers, *downs)


def front_body(
    taps_count,
    extended,
    small,
    gain,
    residual_in,
    out_weight,
    after,
    normal,
    weight,
    residual,
    mixed,
    activated,
    arrivals,
):
    fetch_weight = pltpu.make_async_copy(out_weight, weight, arrivals.at[0])
    fetch_residual = pltpu.make_async_copy(residual_in, residual, arrivals.at[1])
    fetch_weight.start()
    fetch_residual.start()
    row_count, chan_count = mixed.shape
    model_width = after.shape[1]
    lanes = min(128, chan_count)
    piece = 32 if row_count % 32 == 0 else row_count

    def convolve(index, carry):
        here = pl.ds(pl.multiple_of(index * lanes, lanes), lanes)
        total = jnp.zeros((row_count, lanes), jnp.float32) + small[taps_count : taps_count + 1, here]
        for tap_index in range(taps_count):
            total = (
                total
                + small[tap_index : tap_index + 1, here]
                * extended[tap_index : tap_index + row_count, here]
            )
        mixed[:, here] = total
        return carry

    lax.fori_loop(0, chan_count // lanes, convolve, 0)
    scale = small[taps_count + 1 : taps_count + 2, :]
    shift = small[taps_count + 2 : taps_count + 3, :]

    def normalise(index, carry):
        here = pl.ds(pl.multiple_of(index * piece, piece), piece)
        values = mixed[here, :]
        center = jnp.sum(values, 1, keepdims=True) / chan_count
        spread = jnp.sum(values * values, 1, keepdims=True) / chan_count - center * center
        normed = (values - center) * lax.rsqrt(spread + 1e-06) * scale + shift
        activated[here, :] = (normed * jax.nn.sigmoid(normed)).astype(jnp.bfloat16)
        return carry

    lax.fori_loop(0, row_count // piece, normalise, 0)
    fetch_weight.wait()
    fetch_residual.wait()
    width = min(512, model_width)
    squares = jnp.zeros((row_count, 1), jnp.float32)
    for start in range(0, model_width, width):
        here = slice(start, start + width)
        product = jnp.dot(activated[...], weight[:, here], preferred_element_type=jnp.float32)
        rounded = (residual[:, here].astype(jnp.float32) + product).astype(jnp.bfloat16)
        after[:, here] = rounded
        again = rounded.astype(jnp.float32)
        squares = squares + jnp.sum(again * again, 1, keepdims=True)
    factor = lax.rsqrt(squares / model_width + 1e-06)
    for start in range(0, model_width, width):
        here = slice(start, start + width)
        value = after[:, here].astype(jnp.float32) * factor * gain[:, here]
        normal[:, here] = value.astype(jnp.bfloat16)


def front_call(taps_count, extended, small, gain, residual_in, out_weight):
    row_count, model_width = residual_in.shape
    chan_count = extended.shape[1]
    inside = pl.BlockSpec(memory_space=pltpu.VMEM)
    outside = pl.BlockSpec(memory_space=pl.ANY)
    result = jax.ShapeDtypeStruct((row_count, model_width), jnp.bfloat16)
    return pl.pallas_call(
        functools.partial(front_body, taps_count),
        in_specs=[inside, inside, inside, outside, outside],
        out_specs=[inside, inside],
        out_shape=[result, result],
        scratch_shapes=[
            pltpu.VMEM(out_weight.shape, jnp.bfloat16),
            pltpu.VMEM((row_count, model_width), jnp.bfloat16),
            pltpu.VMEM((row_count, chan_count), jnp.float32),
            pltpu.VMEM((row_count, chan_count), jnp.bfloat16),
            pltpu.SemaphoreType.DMA((2,)),
        ],
        cost_estimate=pl.CostEstimate(
            flops=2 * row_count * chan_count * (model_width + taps_count),
            bytes_accessed=2 * chan_count * model_width + 8 * row_count * model_width,
            transcendentals=row_count * chan_count,
        ),
        name="front_rows",
    )(extended, small, gain, residual_in, out_weight)


def on_device(
    residual_in,
    conv_values,
    conv_gates,
    conv_kernel,
    conv_bias,
    chan_gain,
    chan_shift,
    out_weight,
    norm_gain,
    route_ids,
    route_weights,
    expert_gate,
    expert_up,
    expert_down,
):
    taps_count = conv_kernel.shape[0]
    tok_count, local_chan = conv_values.shape
    tp_count = lax.axis_size("tp")
    row_count = tok_count // tp_count
    halo = taps_count - 1
    place = lax.axis_index("tp")
    sp_count = lax.axis_size("sp")
    gated = (
        conv_values.astype(jnp.float32) * jax.nn.sigmoid(conv_gates.astype(jnp.float32))
    ).astype(jnp.bfloat16)
    small = jnp.concatenate(
        [conv_kernel, conv_bias[None, :], chan_gain[None, :], chan_shift[None, :]], 0
    )
    padded = jnp.concatenate([jnp.zeros((halo, local_chan), jnp.bfloat16), gated], 0)

    def window(member):
        return lax.dynamic_slice_in_dim(padded, member * row_count, row_count + halo, 0)

    rows_by_source, small_by_source = ([window(place)], [small])
    for shift in range(1, tp_count):
        turn = [(source, (source + shift) % tp_count) for source in range(tp_count)]
        rows_by_source.append(lax.ppermute(window((place + shift) % tp_count), "tp", turn))
        small_by_source.append(lax.ppermute(small, "tp", turn))
    last = gated[tok_count - halo :]
    earlier = []
    for channel in range(tp_count):
        pairs = [
            (source * tp_count + channel, (source + 1) * tp_count) for source in range(sp_count - 1)
        ]
        earlier.append(lax.ppermute(last, ("sp", "tp"), pairs))

    def in_order(pieces):
        ordered = []
        for channel in range(tp_count):
            chosen = pieces[0]
            for shift in range(1, tp_count):
                chosen = jnp.where((place - shift) % tp_count == channel, pieces[shift], chosen)
            ordered.append(chosen)
        return ordered

    columns = []
    for rows, before_rows in zip(in_order(rows_by_source), earlier):
        first = rows[:halo].astype(jnp.float32) + before_rows.astype(jnp.float32)
        columns.append(jnp.concatenate([first, rows[halo:].astype(jnp.float32)], 0))
    extended = jnp.concatenate(columns, 1)
    after_mix, normal_rows = front_call(
        taps_count,
        extended,
        jnp.concatenate(in_order(small_by_source), 1),
        norm_gain[None, :],
        residual_in,
        out_weight,
    )
    after_f = after_mix.astype(jnp.float32)
    model_width = normal_rows.shape[1]
    experts_all = expert_gate.shape[0] * lax.axis_size("sp")
    choose_count = route_ids.shape[1]
    slot_cap = max(2, (2 * choose_count * row_count + experts_all - 1) // experts_all)
    onehot = (
        route_ids.reshape(-1)[:, None] == jnp.arange(experts_all, dtype=jnp.int32)[None, :]
    ).astype(jnp.int32)
    before = jnp.cumsum(onehot, 0) - onehot
    ranking = jnp.sum(before * onehot, 1).reshape(row_count, choose_count)
    slot_ids = route_ids * slot_cap + ranking
    half = sp_count // 2
    across = [(source, (source + half) % sp_count) for source in range(sp_count)]
    groups = [list(range(start, start + half)) for start in range(0, sp_count, half)]
    exchange = functools.partial(
        lax.all_to_all,
        axis_name="sp",
        split_axis=0,
        concat_axis=0,
        tiled=True,
        axis_index_groups=groups,
    )
    held = (expert_gate[0], expert_up[0], expert_down[0])
    weights = [held]
    for shift in range(1, tp_count):
        turn = [(source, (source + shift) % tp_count) for source in range(tp_count)]
        weights.append(tuple(lax.ppermute(piece, "tp", turn) for piece in held))
    gates, uppers, downs = zip(*weights)
    their_rows = lax.ppermute(normal_rows, "sp", across)
    packed = jnp.concatenate([slot_ids.astype(jnp.float32), route_weights], 1)
    packed, normal_rows = lax.optimization_barrier((packed, normal_rows))
    their_packed = lax.ppermute(packed, "sp", across)
    their_slots = their_packed[:, :choose_count].astype(jnp.int32)
    their_weights = their_packed[:, choose_count:]
    local = half * slot_cap
    base = (lax.axis_index("sp") // half) * local

    def sent_out(rows, slots):
        positions = base + lax.broadcasted_iota(jnp.int32, (local, 1, 1), 0)
        dispatch = jnp.any(positions == slots[None, :, :], axis=2).astype(jnp.bfloat16)
        sendable = jnp.dot(dispatch, rows, preferred_element_type=jnp.float32)
        return exchange(sendable.astype(jnp.bfloat16).reshape(half, slot_cap, model_width))

    def worked(rows):
        return expert_call(rows.reshape(local, model_width), gates, uppers, downs)

    def sent_back(rows):
        return exchange(rows.reshape(half, slot_cap, model_width)).reshape(local, model_width)

    def weighted(results, slots, scale):
        positions = base + lax.broadcasted_iota(jnp.int32, (1, local), 1)
        total = 0.0
        for choice in range(choose_count):
            chosen = (positions == slots[:, choice : choice + 1]).astype(jnp.bfloat16)
            picked = jnp.dot(chosen, results, preferred_element_type=jnp.float32)
            total = total + scale[:, choice : choice + 1] * picked
        return total

    own_in = sent_out(normal_rows, slot_ids)
    own_in, their_rows = lax.optimization_barrier((own_in, their_rows))
    their_in = sent_out(their_rows, their_slots)
    own_result = worked(own_in)
    own_result, their_in = lax.optimization_barrier((own_result, their_in))
    own_out = sent_back(own_result)
    own_out, their_result = lax.optimization_barrier((own_out, worked(their_in)))
    their_out = sent_back(their_result)
    their_sum = weighted(their_out, their_slots, their_weights).astype(jnp.bfloat16)
    returned = lax.ppermute(their_sum, "sp", across).astype(jnp.float32)
    combined = after_f + weighted(own_out, slot_ids, route_weights) + returned
    return combined.astype(jnp.bfloat16)


def solution(mesh):
    placed = (
        P(("sp", "tp"), None),
        P("sp", "tp"),
        P("sp", "tp"),
        P(None, "tp"),
        P("tp"),
        P("tp"),
        P("tp"),
        P(),
        P(),
        P(("sp", "tp"), None),
        P(("sp", "tp"), None),
        P("sp", None, "tp"),
        P("sp", None, "tp"),
        P("sp", "tp", None),
    )

    return jax.shard_map(
        on_device, mesh=mesh, in_specs=placed, out_specs=P(("sp", "tp"), None), check_vma=False
    )
```

time: 228 us -> 188 us (0.82); the launches traced: 227 us -> 185 us
  waiting for transfers between devices: 141 us -> 91.6 us
  Pallas kernels: 0 us -> 44.9 us
  matrix products: 51.8 us -> 8.36 us
  starting transfers between devices: 15.5 us -> 32.1 us
  blocking collectives: 6.65 us -> 0 us
  local copies, waits for them, and re-layouts: 4.94 us -> 2.12 us
    all_to_all x2 -> x4, waiting for transfers between devices: 141 us -> 20.6 us  [the longest x2 20.1 us: sent_back(): exchange(rows.reshape(half, slot_cap, model_width))]
    ppermute x4 -> x10, waiting for transfers between devices: 0.01 us -> 71 us  [the longest x1 34.4 us: on_device(): their_rows = lax.ppermute(normal_rows, 'sp', across)]
    pallas_call x0 -> x3, Pallas kernels: none -> 44.9 us  [the longest x2 36.8 us: expert_call(): pl.pallas_call(functools.partial(expert_body, count, own_steps), grid=(fi...]
    dot_general x8 -> x6, matrix products: 51.8 us -> 8.36 us  [the longest x2 4.73 us: sent_out(): sendable = jnp.dot(dispatch, rows, preferred_element_type=jnp.float32)]
    all_to_all x2 -> x4, starting transfers between devices: 11.5 us -> 21.4 us  [the longest x2 11.1 us: sent_out(): exchange(sendable.astype(jnp.bfloat16).reshape(half, slot_cap, model_width))]
    ppermute x4 -> x10, starting transfers between devices: 4.04 us -> 10.7 us  [the longest x2 4.69 us: on_device(): earlier.append(lax.ppermute(last, ('sp', 'tp'), pairs))]
    all_to_all x1 -> x0, blocking collectives: 4.05 us -> none  [on_device(): lax.all_to_all(activated, 'tp', split_axis=0, concat_axis=1, tiled=True)]
    reduce_sum x1 -> x0, other arithmetic: 3.83 us -> none  [on_device(): row_total = jnp.sum(mixed, 1)]
  transfers between devices with their start and end apart: 6 -> 14, of which waited for: 2 -> 6; matrix products, arithmetic and copies ran while one was open for 15% -> 3% of each run, Pallas kernels for 0% -> 20%
where the time goes in v2:
time: 188 us; the launch traced here: 185 us
  waiting for transfers between devices  91.6 us (49%)
  Pallas kernels  44.9 us (24%)
  starting transfers between devices  32.1 us (17%)
  matrix products  8.36 us (4%)
  other arithmetic  5.52 us (3%)
  local copies, waits for them, and re-layouts  2.12 us (1%)
    pallas_call x2, Pallas kernels, expert_call(): pl.pallas_call(functools.partial(expert_body, count, own_steps), grid=(fi...  36.8 us
    ppermute x1, waiting for transfers between devices, on_device(): their_rows = lax.ppermute(normal_rows, 'sp', across)  34.4 us
    ppermute x1, waiting for transfers between devices, on_device(): returned = lax.ppermute(their_sum, 'sp', across).astype(jnp.float32)  32.6 us
    all_to_all x2, waiting for transfers between devices, sent_back(): exchange(rows.reshape(half, slot_cap, model_width))  20.1 us
    all_to_all x2, starting transfers between devices, sent_out(): exchange(sendable.astype(jnp.bfloat16).reshape(half, slot_cap, model_width))  11.1 us
    all_to_all x2, starting transfers between devices, sent_back(): exchange(rows.reshape(half, slot_cap, model_width))  10.3 us
    pallas_call x1, Pallas kernels, front_call(): pl.pallas_call(functools.partial(front_body, taps_count), in_specs=[insid...  8.06 us
    dot_general x2, matrix products, sent_out(): sendable = jnp.dot(dispatch, rows, preferred_element_type=jnp.float32)  4.73 us
  transfers between devices with their start and end apart: 14, of which 6 were waited for; matrix products, arithmetic and copies ran while one was open for 3% of the time, Pallas kernels for 20%

profile of v2, /device:TPU:14, one launch (start us, length us, event | category | flops | bytes accessed | tf_op | source)
XLA Modules:
  0.0 184.9 jit_solution(13324463273298139273)
XLA Ops:
  0.0 1.4 multiply_convert_fusion
  1.5 1.3 collective-permute-start.2
  2.8 3.4 %collective-permute-start.1 = (bf16[30,512]{1,0:T(8,128)(2,1)S(1)}, bf16[30,512]{1,0:T(8,128)(2,1)S(1)}, u32[]{:S(2)}, u32[]{:S(2)}) collective-permute-start(bf16[30,512]{1,0:T(8,128)(2,1)S(1)} %slice.68), channel_id=1, source_target_pairs={{0,2},{2,4},{4,6},{6,8},{8,10},{10,12},{12,14},{14,16},{16,18},{18... | collective-permute-start | bytes 92168 | tf_op jit(solution)/shard_map/ppermute | solution.py:218
  6.2 0.9 pad_maximum_fusion.1
  8.2 0.9 reduce-window.6
  10.8 1.0 maximum_maximum_fusion.extended
  11.8 8.1 %front_rows.1 = (bf16[192,2048]{1,0:T(8,128)(2,1)}, bf16[192,2048]{1,0:T(8,128)(2,1)}) custom-call(f32[222,1024]{1,0:T(8,128)} %maximum_maximum_fusion.extended, f32[34,1024]{1,0:T(8,128)} %pad_maximum_fusion.small, f32[1,2048]{1,0:T(1,128)} %bitcast.59, bf16[192,2048]{1,0:T(8,128)(2,1)} %residual_in.1, bf16[1024,2048]{1,0:T(8,128)(2,1)} %out_weight.1), custom_call_target="tpu_custom_call" | custom-call | flops 817496064 | bytes 7340032 | tf_op jit(solution)/shard_map/front_rows/pallas_call | solution.py:152
  20.4 4.0 %collective-permute-done.8 = f32[192,4]{0,1:T(4,128)S(1)} collective-permute-done((f32[192,4]{0,1:T(4,128)S(1)}, f32[192,4]{0,1:T(4,128)S(1)}, u32[]{:S(2)}, u32[]{:S(2)}) %collective-permute-start.8) | collective-permute-done | bytes 3104 | tf_op jit(solution)/shard_map/ppermute | solution.py:273
  24.7 2.9 %convolution_convert_fusion.1 = bf16[384,2048]{1,0:T(8,128)(2,1)} fusion(pred[384,192]{0,1:T(8,128)(4,1)S(1)} %get-tuple-element.26, bf16[192,2048]{1,0:T(8,128)(2,1)} %get-tuple-element.17), kind=kOutput, calls=%fused_computation.1 | convolution fusion | flops 302776320 | bytes 2433024 | tf_op jit(solution)/shard_map/dot_general | solution.py:282
  27.6 5.2 %all-to-all-start = ((bf16[8,48,2048]{2,1,0:T(8,128)(2,1)}), bf16[8,48,2048]{2,1,0:T(8,128)(2,1)S(1)}, u32[]{:S(2)}, u32[]{:S(2)}) async-start(bf16[8,48,2048]{2,1,0:T(8,128)(2,1)} %bitcast.7), calls=%async_computation | async-start | bytes 3145728 | tf_op jit(solution)/shard_map/all_to_all | solution.py:283
  33.4 1.7 collective-permute-start.4
  35.0 34.4 %collective-permute-done.4 = bf16[192,2048]{1,0:T(8,128)(2,1)S(1)} collective-permute-done((bf16[192,2048]{1,0:T(8,128)(2,1)S(1)}, bf16[192,2048]{1,0:T(8,128)(2,1)S(1)}, u32[]{:S(2)}, u32[]{:S(2)}) %collective-permute-start.4) | collective-permute-done | bytes 786464 | tf_op jit(solution)/shard_map/ppermute | solution.py:270
  69.4 1.8 convolution_convert_fusion
  71.2 5.9 %all-to-all-start.1 = ((bf16[8,48,2048]{2,1,0:T(8,128)(2,1)}), bf16[8,48,2048]{2,1,0:T(8,128)(2,1)S(1)}, u32[]{:S(2)}, u32[]{:S(2)}) async-start(bf16[8,48,2048]{2,1,0:T(8,128)(2,1)} %bitcast.12), calls=%async_computation.1 | async-start | bytes 3145728 | tf_op jit(solution)/shard_map/all_to_all | solution.py:283
  77.1 18.4 %expert_rows.2 = bf16[384,2048]{1,0:T(8,128)(2,1)} custom-call(bf16[384,2048]{1,0:T(8,128)(2,1)} %bitcast.55, bf16[2048,1024]{1,0:T(8,128)(2,1)} %bitcast.76, bf16[2048,1024]{1,0:T(8,128)(2,1)} %collective-permute-done.5.refs_1_, bf16[2048,1024]{1,0:T(8,128)(2,1)} %bitcast.79, bf16[2048,1024]{1,0:T(8,128)(2,1)} %collective-permute-done.6.refs_3_, ...), custom_call_target="tpu_custom_call" | custom-call | flops 9663676416 | bytes 25165824 | tf_op jit(solution)/shard_map/expert_rows/pallas_call | solution.py:57
  96.0 1.1 copy-done.1
  97.2 5.1 %all-to-all-start.2 = ((bf16[8,48,2048]{2,1,0:T(8,128)(2,1)}), bf16[8,48,2048]{2,1,0:T(8,128)(2,1)S(1)}, u32[]{:S(2)}, u32[]{:S(2)}) async-start(bf16[8,48,2048]{2,1,0:T(8,128)(2,1)} %bitcast.58), calls=%async_computation.2 | async-start | bytes 3145728 | tf_op jit(solution)/shard_map/all_to_all | solution.py:289
  102.3 18.5 %expert_rows.3 = bf16[384,2048]{1,0:T(8,128)(2,1)} custom-call(bf16[384,2048]{1,0:T(8,128)(2,1)} %bitcast.56, bf16[2048,1024]{1,0:T(8,128)(2,1)} %bitcast.77, bf16[2048,1024]{1,0:T(8,128)(2,1)} %collective-permute-done.5.refs_1_, bf16[2048,1024]{1,0:T(8,128)(2,1)} %bitcast.80, bf16[2048,1024]{1,0:T(8,128)(2,1)} %collective-permute-done.6.refs_3_, ...), custom_call_target="tpu_custom_call" | custom-call | flops 9663676416 | bytes 25165824 | tf_op jit(solution)/shard_map/expert_rows/pallas_call | solution.py:57
  120.8 1.0 all-to-all-done.2
  121.8 5.2 %all-to-all-start.3 = ((bf16[8,48,2048]{2,1,0:T(8,128)(2,1)}), bf16[8,48,2048]{2,1,0:T(8,128)(2,1)S(1)}, u32[]{:S(2)}, u32[]{:S(2)}) async-start(bf16[8,48,2048]{2,1,0:T(8,128)(2,1)} %bitcast.57), calls=%async_computation.3 | async-start | bytes 3145728 | tf_op jit(solution)/shard_map/all_to_all | solution.py:289
  127.0 19.1 %all-to-all-done.3 = bf16[8,48,2048]{2,1,0:T(8,128)(2,1)S(1)} async-done(((bf16[8,48,2048]{2,1,0:T(8,128)(2,1)}), bf16[8,48,2048]{2,1,0:T(8,128)(2,1)S(1)}, u32[]{:S(2)}, u32[]{:S(2)}) %all-to-all-start.3) | async-done | bytes 1572896 | tf_op jit(solution)/shard_map/all_to_all | solution.py:289
  147.4 2.6 %collective-permute-start.9 = (bf16[192,2048]{1,0:T(8,128)(2,1)S(1)}, bf16[192,2048]{1,0:T(8,128)(2,1)S(1)}, u32[]{:S(2)}, u32[]{:S(2)}) collective-permute-start(bf16[192,2048]{1,0:T(8,128)(2,1)S(1)} %add_convert_fusion), channel_id=1, source_target_pairs={{0,16},{2,18},{4,20},{6,22},{8,24},{10,26},{12,28},{14,30},{16,0},... | collective-permute-start | bytes 2359304 | tf_op jit(solution)/shard_map/ppermute | solution.py:309
  150.7 32.6 %collective-permute-done.9 = bf16[192,2048]{1,0:T(8,128)(2,1)S(1)} collective-permute-done((bf16[192,2048]{1,0:T(8,128)(2,1)S(1)}, bf16[192,2048]{1,0:T(8,128)(2,1)S(1)}, u32[]{:S(2)}, u32[]{:S(2)}) %collective-permute-start.9) | collective-permute-done | bytes 786464 | tf_op jit(solution)/shard_map/ppermute | solution.py:309
  183.2 1.7 fusion.3
  (63 shorter events, 6.5 us)
Async XLA Ops:
  0.0 9.7 %copy-start.4 = (f32[31,512]{1,0:T(8,128)S(1)}, f32[31,512]{1,0:T(8,128)}, u32[]{:S(2)}) copy-start(f32[31,512]{1,0:T(8,128)} %param.17) | copy-start | bytes 190468
  0.0 9.7 %copy-start.5 = (f32[512]{0:T(512)S(1)}, f32[512]{0:T(512)}, u32[]{:S(2)}) copy-start(f32[512]{0:T(512)} %param.20) | copy-start | bytes 6148
  0.0 9.8 %copy-start.6 = (f32[512]{0:T(512)S(1)}, f32[512]{0:T(512)}, u32[]{:S(2)}) copy-start(f32[512]{0:T(512)} %param.19) | copy-start | bytes 6148
  0.0 9.8 %copy-start.7 = (f32[512]{0:T(512)S(1)}, f32[512]{0:T(512)}, u32[]{:S(2)}) copy-start(f32[512]{0:T(512)} %param.18) | copy-start | bytes 6148
  0.0 7.8 %copy-start.8 = (s32[192,2]{0,1:T(2,128)S(1)}, s32[192,2]{0,1:T(2,128)}, u32[]{:S(2)}) copy-start(s32[192,2]{0,1:T(2,128)} %param.23) | copy-start | bytes 4612
  0.0 9.7 %copy-start.9 = (f32[192,2]{0,1:T(2,128)S(1)}, f32[192,2]{0,1:T(2,128)}, u32[]{:S(2)}) copy-start(f32[192,2]{0,1:T(2,128)} %param.24) | copy-start | bytes 4612
  1.5 9.3 %collective-permute-start.2 = (bf16[30,512]{1,0:T(8,128)(2,1)S(1)}, bf16[30,512]{1,0:T(8,128)(2,1)S(1)}, u32[]{:S(2)}, u32[]{:S(2)}) collective-permute-start(bf16[30,512]{1,0:T(8,128)(2,1)S(1)} %slice.68), channel_id=1, source_target_pairs={{1,2},{3,4},{5,6},{7,8},{9,10},{11,12},{13,14},{15,16},{17,18},{19... | collective-permute-start | bytes 92168 | tf_op jit(solution)/shard_map/ppermute | solution.py:218
  2.8 8.0 %collective-permute-start.1 = (bf16[30,512]{1,0:T(8,128)(2,1)S(1)}, bf16[30,512]{1,0:T(8,128)(2,1)S(1)}, u32[]{:S(2)}, u32[]{:S(2)}) collective-permute-start(bf16[30,512]{1,0:T(8,128)(2,1)S(1)} %slice.68), channel_id=1, source_target_pairs={{0,2},{2,4},{4,6},{6,8},{8,10},{10,12},{12,14},{14,16},{16,18},{18... | collective-permute-start | bytes 92168 | tf_op jit(solution)/shard_map/ppermute | solution.py:218
  7.1 2.6 %collective-permute-start.3 = (f32[34,512]{1,0:T(8,128)S(1)}, f32[34,512]{1,0:T(8,128)S(1)}, u32[]{:S(2)}, u32[]{:S(2)}) collective-permute-start(f32[34,512]{1,0:T(8,128)S(1)} %pad_maximum_fusion.1), channel_id=1, source_target_pairs={{0,1},{1,0},{2,3},{3,2},{4,5},{5,4},{6,7},{7,6},{8,9},{9,8},{10,11... | collective-permute-start | bytes 208904 | tf_op jit(solution)/shard_map/ppermute | solution.py:211
  7.3 3.2 %collective-permute-start = (bf16[222,512]{1,0:T(8,128)(2,1)S(1)}, bf16[222,512]{1,0:T(8,128)(2,1)S(1)}, u32[]{:S(2)}, u32[]{:S(2)}) collective-permute-start(bf16[222,512]{1,0:T(8,128)(2,1)S(1)} %pad_dynamic-slice_fusion.1), channel_id=1, source_target_pairs={{0,1},{1,0},{2,3},{3,2},{4,5},{5,4},{6,7},{7,6},{8,9},{9,8},{10,11... | collective-permute-start | bytes 681992 | tf_op jit(solution)/shard_map/ppermute | solution.py:210
  19.9 4.6 %collective-permute-start.8 = (f32[192,4]{0,1:T(4,128)S(1)}, f32[192,4]{0,1:T(4,128)S(1)}, u32[]{:S(2)}, u32[]{:S(2)}) collective-permute-start(f32[192,4]{0,1:T(4,128)S(1)} %pad_maximum_fusion.2), channel_id=1, source_target_pairs={{0,16},{2,18},{4,20},{6,22},{8,24},{10,26},{12,28},{14,30},{16,0},... | collective-permute-start | bytes 9224 | tf_op jit(solution)/shard_map/ppermute | solution.py:273
  27.6 5.7 %copy-start.3 = (bf16[192,2048]{1,0:T(8,128)(2,1)S(1)}, bf16[192,2048]{1,0:T(8,128)(2,1)}, u32[]{:S(2)}) copy-start(bf16[192,2048]{1,0:T(8,128)(2,1)} %get-tuple-element.17) | copy-start | bytes 2359300
  27.6 41.8 %all-to-all-start = ((bf16[8,48,2048]{2,1,0:T(8,128)(2,1)}), bf16[8,48,2048]{2,1,0:T(8,128)(2,1)S(1)}, u32[]{:S(2)}, u32[]{:S(2)}) async-start(bf16[8,48,2048]{2,1,0:T(8,128)(2,1)} %bitcast.7), calls=%async_computation | async-start | bytes 3145728 | tf_op jit(solution)/shard_map/all_to_all | solution.py:283
  32.8 44.3 %collective-permute-start.5 = (bf16[2048,1024]{1,0:T(8,128)(2,1)}, bf16[2048,1024]{1,0:T(8,128)(2,1)}, u32[]{:S(2)}, u32[]{:S(2)}) collective-permute-start(bf16[2048,1024]{1,0:T(8,128)(2,1)} %bitcast.75), channel_id=1, source_target_pairs={{0,1},{1,0},{2,3},{3,2},{4,5},{5,4},{6,7},{7,6},{8,9},{9,8},{10,11... | collective-permute-start | bytes 12582920 | tf_op jit(solution)/shard_map/ppermute | solution.py:268
  32.8 44.3 %collective-permute-start.6 = (bf16[2048,1024]{1,0:T(8,128)(2,1)}, bf16[2048,1024]{1,0:T(8,128)(2,1)}, u32[]{:S(2)}, u32[]{:S(2)}) collective-permute-start(bf16[2048,1024]{1,0:T(8,128)(2,1)} %bitcast.78), channel_id=1, source_target_pairs={{0,1},{1,0},{2,3},{3,2},{4,5},{5,4},{6,7},{7,6},{8,9},{9,8},{10,11... | collective-permute-start | bytes 12582920 | tf_op jit(solution)/shard_map/ppermute | solution.py:268
  33.3 43.8 %collective-permute-start.7 = (bf16[1024,2048]{1,0:T(8,128)(2,1)}, bf16[1024,2048]{1,0:T(8,128)(2,1)}, u32[]{:S(2)}, u32[]{:S(2)}) collective-permute-start(bf16[1024,2048]{1,0:T(8,128)(2,1)} %bitcast.81), channel_id=1, source_target_pairs={{0,1},{1,0},{2,3},{3,2},{4,5},{5,4},{6,7},{7,6},{8,9},{9,8},{10,11... | collective-permute-start | bytes 12582920 | tf_op jit(solution)/shard_map/ppermute | solution.py:268
  33.4 36.0 %collective-permute-start.4 = (bf16[192,2048]{1,0:T(8,128)(2,1)S(1)}, bf16[192,2048]{1,0:T(8,128)(2,1)S(1)}, u32[]{:S(2)}, u32[]{:S(2)}) collective-permute-start(bf16[192,2048]{1,0:T(8,128)(2,1)S(1)} %copy-done.3), channel_id=1, source_target_pairs={{0,16},{2,18},{4,20},{6,22},{8,24},{10,26},{12,28},{14,30},{16,0},... | collective-permute-start | bytes 2359304 | tf_op jit(solution)/shard_map/ppermute | solution.py:270
  69.4 1.8 copy-start
  71.2 24.8 %all-to-all-start.1 = ((bf16[8,48,2048]{2,1,0:T(8,128)(2,1)}), bf16[8,48,2048]{2,1,0:T(8,128)(2,1)S(1)}, u32[]{:S(2)}, u32[]{:S(2)}) async-start(bf16[8,48,2048]{2,1,0:T(8,128)(2,1)} %bitcast.12), calls=%async_computation.1 | async-start | bytes 3145728 | tf_op jit(solution)/shard_map/all_to_all | solution.py:283
  96.0 1.2 copy-start.1
  97.2 24.6 %all-to-all-start.2 = ((bf16[8,48,2048]{2,1,0:T(8,128)(2,1)}), bf16[8,48,2048]{2,1,0:T(8,128)(2,1)S(1)}, u32[]{:S(2)}, u32[]{:S(2)}) async-start(bf16[8,48,2048]{2,1,0:T(8,128)(2,1)} %bitcast.58), calls=%async_computation.2 | async-start | bytes 3145728 | tf_op jit(solution)/shard_map/all_to_all | solution.py:289
  121.8 24.3 %all-to-all-start.3 = ((bf16[8,48,2048]{2,1,0:T(8,128)(2,1)}), bf16[8,48,2048]{2,1,0:T(8,128)(2,1)S(1)}, u32[]{:S(2)}, u32[]{:S(2)}) async-start(bf16[8,48,2048]{2,1,0:T(8,128)(2,1)} %bitcast.57), calls=%async_computation.3 | async-start | bytes 3145728 | tf_op jit(solution)/shard_map/all_to_all | solution.py:289
  147.4 35.9 %collective-permute-start.9 = (bf16[192,2048]{1,0:T(8,128)(2,1)S(1)}, bf16[192,2048]{1,0:T(8,128)(2,1)S(1)}, u32[]{:S(2)}, u32[]{:S(2)}) collective-permute-start(bf16[192,2048]{1,0:T(8,128)(2,1)S(1)} %add_convert_fusion), channel_id=1, source_target_pairs={{0,16},{2,18},{4,20},{6,22},{8,24},{10,26},{12,28},{14,30},{16,0},... | collective-permute-start | bytes 2359304 | tf_op jit(solution)/shard_map/ppermute | solution.py:309
  150.0 33.2 %copy-start.2 = (bf16[192,2048]{1,0:T(8,128)(2,1)S(1)}, bf16[192,2048]{1,0:T(8,128)(2,1)}, u32[]{:S(2)}) copy-start(bf16[192,2048]{1,0:T(8,128)(2,1)} %get-tuple-element.15) | copy-start | bytes 2359300

commit v3 on v2

v3 whole, which is shorter than its diff:
```python
import functools

import jax
import jax.numpy as jnp
from jax import lax
from jax.experimental import pallas as pl
from jax.experimental.pallas import tpu as pltpu
from jax.sharding import PartitionSpec as P


def expert_body(count, own_steps, out_steps, rows, *refs):
    gates, uppers, downs = (refs[:count], refs[count : 2 * count], refs[2 * count : 3 * count])
    outs, hidden = (refs[3 * count : -1], refs[-1])
    step = pl.program_id(0)
    width = gates[0].shape[1]
    for part in range(count):

        @pl.when((step >= part * own_steps) & (step < (part + 1) * own_steps))
        def _(part=part):
            gate = jnp.dot(rows[...], gates[part][...], preferred_element_type=jnp.float32)
            upper = jnp.dot(rows[...], uppers[part][...], preferred_element_type=jnp.float32)
            value = (gate * jax.nn.sigmoid(gate) * upper).astype(jnp.bfloat16)
            hidden[step] = value

    first_steps = count * own_steps

    @pl.when(step >= first_steps)
    def _():
        total = None
        for part in range(count):
            for piece in range(own_steps):
                product = jnp.dot(
                    hidden[part * own_steps + piece],
                    downs[part][piece * width : (piece + 1) * width, :],
                    preferred_element_type=jnp.float32,
                )
                total = product if total is None else total + product
        each = out_steps // len(outs)
        for index, out in enumerate(outs):

            @pl.when((step - first_steps) // each == index)
            def _(out=out):
                out[...] = total.astype(jnp.bfloat16)


def expert_call(rows, gates, uppers, downs, parts):
    count = len(gates)
    row_total, model_width = rows.shape
    own_hidden = gates[0].shape[1]
    width = min(512, own_hidden)
    own_steps = own_hidden // width
    first_steps = count * own_steps
    out_steps = model_width // width
    each = out_steps // parts

    def inward(part):
        return pl.BlockSpec(
            (model_width, width),
            lambda i: (0, jnp.clip(i - part * own_steps, 0, own_steps - 1)),
        )

    outward = pl.BlockSpec(
        (own_hidden, width), lambda i: (0, jnp.clip(i - first_steps, 0, out_steps - 1))
    )
    return pl.pallas_call(
        functools.partial(expert_body, count, own_steps, out_steps),
        grid=(first_steps + out_steps,),
        in_specs=[pl.BlockSpec(memory_space=pltpu.VMEM)]
        + [inward(part) for part in range(count)] * 2
        + [outward] * count,
        out_specs=[
            pl.BlockSpec(
                (row_total, width),
                lambda i, part=part: (0, jnp.clip(i - first_steps - part * each, 0, each - 1)),
            )
            for part in range(parts)
        ],
        out_shape=[jax.ShapeDtypeStruct((row_total, model_width // parts), jnp.bfloat16)] * parts,
        scratch_shapes=[pltpu.VMEM((first_steps, row_total, width), jnp.bfloat16)],
        compiler_params=pltpu.CompilerParams(dimension_semantics=("arbitrary",)),
        cost_estimate=pl.CostEstimate(
            flops=6 * row_total * model_width * own_hidden * count,
            bytes_accessed=6 * model_width * own_hidden * count,
            transcendentals=row_total * own_hidden * count,
        ),
        name="expert_rows",
    )(pltpu.with_memory_space_constraint(rows, pltpu.VMEM), *gates, *uppers, *downs)


def prep_body(experts_all, slot_cap, *refs):
    values, gates, bias, gain, shift, ids, scales = refs[:7]
    last, vectors, packed, arrivals = refs[7:]
    lead = last.shape[0] // 2
    copies = []
    for index, source in enumerate((values, gates)):
        rows = pl.ds(source.shape[0] - lead, lead)
        copies.append(
            pltpu.make_async_copy(
                source.at[rows, :], last.at[pl.ds(index * lead, lead), :], arrivals.at[index]
            )
        )
    for copy in copies:
        copy.start()
    for index, source in enumerate((bias, gain, shift)):
        vectors[index : index + 1, :] = source[...]
    choose_count, row_count = ids.shape
    experts = lax.broadcasted_iota(jnp.int32, (experts_all, row_count), 0)
    named = [experts == ids[choice : choice + 1, :] for choice in range(choose_count)]
    marks = jnp.zeros((experts_all, row_count), jnp.float32)
    for mask in named:
        marks = jnp.where(mask, 1.0, marks)
    rows_down = lax.broadcasted_iota(jnp.int32, (row_count, row_count), 0)
    rows_along = lax.broadcasted_iota(jnp.int32, (row_count, row_count), 1)
    ahead = jnp.where(rows_down < rows_along, 1.0, 0.0).astype(jnp.bfloat16)
    before = jnp.dot(marks.astype(jnp.bfloat16), ahead, preferred_element_type=jnp.float32)
    packed[...] = jnp.zeros(packed.shape, jnp.float32)
    for choice, mask in enumerate(named):
        rank = jnp.sum(jnp.where(mask, before, 0.0), 0, keepdims=True)
        slot = ids[choice : choice + 1, :].astype(jnp.float32) * float(slot_cap) + rank
        packed[choice : choice + 1, :] = slot
        place = choose_count + choice
        packed[place : place + 1, :] = scales[choice : choice + 1, :]
    for copy in copies:
        copy.wait()


def prep_call(lead, experts_all, slot_cap, values, gates, vectors, ids, scales):
    choose_count, row_count = ids.shape
    width = values.shape[1]
    depth = -(-2 * choose_count // 8) * 8
    inside = pl.BlockSpec(memory_space=pltpu.VMEM)
    outside = pl.BlockSpec(memory_space=pl.ANY)
    return pl.pallas_call(
        functools.partial(prep_body, experts_all, slot_cap),
        in_specs=[outside, outside] + [inside] * 5,
        out_specs=[inside] * 3,
        out_shape=[
            jax.ShapeDtypeStruct((2 * lead, width), jnp.bfloat16),
            jax.ShapeDtypeStruct((len(vectors), width), jnp.float32),
            jax.ShapeDtypeStruct((depth, row_count), jnp.float32),
        ],
        scratch_shapes=[pltpu.SemaphoreType.DMA((2,))],
        name="prep_rows",
    )(values, gates, *[vector[None, :] for vector in vectors], ids, scales)


def front_body(taps_count, choose_count, count, lead, *refs):
    place = lax.axis_index("tp")
    values, gates, kernels, vectors, earlier = (
        refs[group * count : (group + 1) * count] for group in range(5)
    )
    slots, gain, residual_in, out_weight = refs[5 * count : 4 + 5 * count]
    after, normal, sendable = refs[4 + 5 * count : 7 + 5 * count]
    extended, taps, weight, residual, mixed, activated, arrivals = refs[7 + 5 * count :]
    fetch_weight = pltpu.make_async_copy(out_weight, weight, arrivals.at[0])
    fetch_residual = pltpu.make_async_copy(residual_in, residual, arrivals.at[1])
    fetch_weight.start()
    fetch_residual.start()
    row_count, chan_count = mixed.shape
    width = chan_count // count
    model_width = after.shape[1]
    lanes = min(128, width)
    piece = 32 if row_count % 32 == 0 else row_count

    def gated(value, gate):
        product = value.astype(jnp.float32) * jax.nn.sigmoid(gate.astype(jnp.float32))
        return product.astype(jnp.bfloat16).astype(jnp.float32)

    for member in range(count):

        @pl.when(place == member)
        def _(member=member):
            start = member * row_count
            for channel in range(count):
                shift = (member - channel) % count
                here = slice(channel * width, (channel + 1) * width)
                if member:
                    rows = slice(start - lead, start)
                    first = gated(values[shift][rows, :], gates[shift][rows, :])
                else:
                    first = gated(earlier[channel][:lead, :], earlier[channel][lead:, :])
                extended[:lead, here] = first
                rows = slice(start, start + row_count)
                extended[lead:, here] = gated(values[shift][rows, :], gates[shift][rows, :])
                taps[:taps_count, here] = kernels[shift][...]
                taps[taps_count:, here] = vectors[shift][...]

    origin = lead - (taps_count - 1)

    def convolve(index, carry):
        here = pl.ds(pl.multiple_of(index * lanes, lanes), lanes)
        total = jnp.zeros((row_count, lanes), jnp.float32) + taps[taps_count : taps_count + 1, here]
        for offset in range(min(8, taps_count)):
            used = range(offset, taps_count, 8)
            reach = row_count + 8 * (len(used) - 1)
            shifted = extended[origin + offset : origin + offset + reach, here]
            for turn, tap_index in enumerate(used):
                total = (
                    total
                    + taps[tap_index : tap_index + 1, here]
                    * shifted[8 * turn : 8 * turn + row_count]
                )
        mixed[:, here] = total
        return carry

    lax.fori_loop(0, chan_count // lanes, convolve, 0)
    scale = taps[taps_count + 1 : taps_count + 2, :]
    offset = taps[taps_count + 2 : taps_count + 3, :]

    def normalise(index, carry):
        here = pl.ds(pl.multiple_of(index * piece, piece), piece)
        held = mixed[here, :]
        center = jnp.sum(held, 1, keepdims=True) / chan_count
        spread = jnp.sum(held * held, 1, keepdims=True) / chan_count - center * center
        normed = (held - center) * lax.rsqrt(spread + 1e-06) * scale + offset
        activated[here, :] = (normed * jax.nn.sigmoid(normed)).astype(jnp.bfloat16)
        return carry

    lax.fori_loop(0, row_count // piece, normalise, 0)
    fetch_weight.wait()
    fetch_residual.wait()
    block = min(512, model_width)
    squares = jnp.zeros((row_count, 1), jnp.float32)
    for start in range(0, model_width, block):
        here = slice(start, start + block)
        product = jnp.dot(activated[...], weight[:, here], preferred_element_type=jnp.float32)
        rounded = (residual[:, here].astype(jnp.float32) + product).astype(jnp.bfloat16)
        after[:, here] = rounded
        again = rounded.astype(jnp.float32)
        squares = squares + jnp.sum(again * again, 1, keepdims=True)
    factor = lax.rsqrt(squares / model_width + 1e-06)
    local = sendable.shape[0]
    half = lax.axis_size("sp") // 2
    base = (lax.axis_index("sp") // half) * local
    positions = base + lax.broadcasted_iota(jnp.int32, (sendable.shape[0], row_count), 0)
    dispatch = jnp.zeros(positions.shape, jnp.float32)
    for choice in range(choose_count):
        slot = slots[choice : choice + 1, :].astype(jnp.int32)
        dispatch = jnp.where(positions == slot, 1.0, dispatch)
    dispatch = dispatch.astype(jnp.bfloat16)
    for start in range(0, model_width, block):
        here = slice(start, start + block)
        value = after[:, here].astype(jnp.float32) * factor * gain[:, here]
        value = value.astype(jnp.bfloat16)
        normal[:, here] = value
        picked = jnp.dot(dispatch, value, preferred_element_type=jnp.float32)
        sendable[:, here] = picked.astype(jnp.bfloat16)


def front_call(
    values,
    gates,
    kernels,
    vectors,
    earlier,
    slots,
    gain,
    residual_in,
    out_weight,
    local,
    choose_count,
):
    count = len(values)
    near = functools.partial(pltpu.with_memory_space_constraint, memory_space=pltpu.VMEM)
    row_count, model_width = residual_in.shape
    chan_count = out_weight.shape[0]
    taps_count = kernels[0].shape[0]
    lead = earlier[0].shape[0] // 2
    inside = pl.BlockSpec(memory_space=pltpu.VMEM)
    outside = pl.BlockSpec(memory_space=pl.ANY)
    result = jax.ShapeDtypeStruct((row_count, model_width), jnp.bfloat16)
    return pl.pallas_call(
        functools.partial(front_body, taps_count, choose_count, count, lead),
        in_specs=[inside] * (5 * count + 2) + [outside, outside],
        out_specs=[inside, inside, inside],
        out_shape=[result, result, jax.ShapeDtypeStruct((local, model_width), jnp.bfloat16)],
        scratch_shapes=[
            pltpu.VMEM((lead + row_count, chan_count), jnp.float32),
            pltpu.VMEM((taps_count + vectors[0].shape[0], chan_count), jnp.float32),
            pltpu.VMEM(out_weight.shape, jnp.bfloat16),
            pltpu.VMEM((row_count, model_width), jnp.bfloat16),
            pltpu.VMEM((row_count, chan_count), jnp.float32),
            pltpu.VMEM((row_count, chan_count), jnp.bfloat16),
            pltpu.SemaphoreType.DMA((2,)),
        ],
        cost_estimate=pl.CostEstimate(
            flops=2 * row_count * chan_count * (model_width + taps_count),
            bytes_accessed=2 * chan_count * model_width + 8 * row_count * model_width,
            transcendentals=2 * row_count * chan_count,
        ),
        name="front_rows",
    )(
        *values[:1],
        *[near(array) for array in values[1:]],
        *gates[:1],
        *[near(array) for array in gates[1:]],
        *kernels[:1],
        *[near(array) for array in kernels[1:]],
        *[near(array) for array in (*vectors, *earlier, slots)],
        gain,
        residual_in,
        out_weight,
    )


def on_device(
    residual_in,
    conv_values,
    conv_gates,
    conv_kernel,
    conv_bias,
    chan_gain,
    chan_shift,
    out_weight,
    norm_gain,
    route_ids,
    route_weights,
    expert_gate,
    expert_up,
    expert_down,
):
    taps_count = conv_kernel.shape[0]
    tok_count, _ = conv_values.shape
    tp_count = lax.axis_size("tp")
    row_count = tok_count // tp_count
    lead = -(-(taps_count - 1) // 16) * 16
    sp_count = lax.axis_size("sp")
    model_width = residual_in.shape[1]
    experts_all = expert_gate.shape[0] * sp_count
    choose_count = route_ids.shape[1]
    slot_cap = max(2, (2 * choose_count * row_count + experts_all - 1) // experts_all)
    last, vectors, packed = prep_call(
        lead,
        experts_all,
        slot_cap,
        conv_values,
        conv_gates,
        (conv_bias, chan_gain, chan_shift),
        route_ids.T,
        route_weights.T,
    )
    shared = [[conv_values], [conv_gates], [conv_kernel], [vectors]]
    for shift in range(1, tp_count):
        turn = [(source, (source + shift) % tp_count) for source in range(tp_count)]
        for held in shared:
            held.append(lax.ppermute(held[0], "tp", turn))
    earlier = []
    for channel in range(tp_count):
        pairs = [
            (source * tp_count + channel, (source + 1) * tp_count) for source in range(sp_count - 1)
        ]
        earlier.append(lax.ppermute(last, ("sp", "tp"), pairs))
    half = sp_count // 2
    local = half * slot_cap
    base = (lax.axis_index("sp") // half) * local
    across = [(source, (source + half) % sp_count) for source in range(sp_count)]
    groups = [list(range(start, start + half)) for start in range(0, sp_count, half)]
    exchange = functools.partial(
        lax.all_to_all,
        axis_name="sp",
        split_axis=0,
        concat_axis=0,
        tiled=True,
        axis_index_groups=groups,
    )
    after_mix, normal_rows, sendable = front_call(
        *shared,
        earlier,
        packed,
        norm_gain[None, :],
        residual_in,
        out_weight,
        local,
        choose_count,
    )
    after_f = after_mix.astype(jnp.float32)
    their_rows = lax.ppermute(normal_rows, "sp", across)
    packed, sendable = lax.optimization_barrier((packed, sendable))
    their_packed = lax.ppermute(packed, "sp", across)
    slot_ids = packed[:choose_count].astype(jnp.int32).T
    their_slots = their_packed[:choose_count].astype(jnp.int32)
    their_weights = their_packed[choose_count : 2 * choose_count].T
    held = (expert_gate[0], expert_up[0], expert_down[0])
    weights = [held]
    for shift in range(1, tp_count):
        turn = [(source, (source + shift) % tp_count) for source in range(tp_count)]
        weights.append(tuple(lax.ppermute(piece, "tp", turn) for piece in held))
    gates, uppers, downs = zip(*weights)

    def worked(rows, parts):
        return expert_call(rows.reshape(local, model_width), gates, uppers, downs, parts)

    def sent_back(rows):
        return exchange(rows.reshape(half, slot_cap, -1)).reshape(local, -1)

    def weighted(results, slots, scale):
        positions = base + lax.broadcasted_iota(jnp.int32, (1, local), 1)
        total = 0.0
        for choice in range(choose_count):
            chosen = (positions == slots[:, choice : choice + 1]).astype(jnp.bfloat16)
            picked = jnp.dot(chosen, results, preferred_element_type=jnp.float32)
            total = total + scale[:, choice : choice + 1] * picked
        return total

    own_in = exchange(sendable.reshape(half, slot_cap, model_width))
    positions = base + lax.broadcasted_iota(jnp.int32, (local, row_count), 0)
    marked = [positions == their_slots[k : k + 1] for k in range(choose_count)]
    dispatch = functools.reduce(jnp.logical_or, marked).astype(jnp.bfloat16)
    their_rows, own_in = lax.optimization_barrier((their_rows, own_in))
    their_send = jnp.dot(dispatch, their_rows, preferred_element_type=jnp.float32)
    their_send = their_send.astype(jnp.bfloat16).reshape(half, slot_cap, model_width)
    their_in = exchange(their_send)
    (own_result,) = worked(own_in, 1)
    own_result, their_in = lax.optimization_barrier((own_result, their_in))
    own_out = sent_back(own_result)
    their_parts = worked(their_in, 1)
    own_out, their_parts = lax.optimization_barrier((own_out, their_parts))
    own_sum = weighted(own_out, slot_ids, route_weights)
    their_out = sent_back(their_parts[0])
    their_sum = weighted(their_out, their_slots.T, their_weights).astype(jnp.bfloat16)
    returned = lax.ppermute(their_sum, "sp", across).astype(jnp.float32)
    combined = after_f + own_sum + returned
    return combined.astype(jnp.bfloat16)


def solution(mesh):
    placed = (
        P(("sp", "tp"), None),
        P("sp", "tp"),
        P("sp", "tp"),
        P(None, "tp"),
        P("tp"),
        P("tp"),
        P("tp"),
        P(),
        P(),
        P(("sp", "tp"), None),
        P(("sp", "tp"), None),
        P("sp", None, "tp"),
        P("sp", None, "tp"),
        P("sp", "tp", None),
    )

    return jax.shard_map(
        on_device, mesh=mesh, in_specs=placed, out_specs=P(("sp", "tp"), None), check_vma=False
    )
```

time: 188 us -> 183 us (0.973)
  other arithmetic: 5.52 us -> 0.71 us
  matrix products: 8.36 us -> 5.45 us
  Pallas kernels: 44.9 us -> 47.1 us
    ppermute x1, waiting for transfers between devices: 34.4 us -> 0.01 us  [on_device(): their_rows = lax.ppermute(normal_rows, 'sp', across)]
    ppermute x1, waiting for transfers between devices: 4.02 us -> 34.9 us  [on_device(): their_packed = lax.ppermute(packed, 'sp', across)]
    dot_general x2 -> x1, matrix products: 4.73 us -> 1.81 us  [on_device(): jnp.dot(dispatch, their_rows, preferred_element_type=jnp.float32)]
    concatenate x4 -> x0, other arithmetic: 2.63 us -> none  [the longest x1 1.03 us: on_device(): extended = jnp.concatenate(columns, 1)]
    pallas_call x3 -> x4, Pallas kernels: 44.9 us -> 47.1 us  [the longest x2 35.8 us: expert_call(): pl.pallas_call(functools.partial(expert_body, count, own_steps, out_steps...]
  transfers between devices with their start and end apart: 14 -> 16, of which waited for: 6 -> 7; matrix products, arithmetic and copies ran while one was open for 3% -> 2% of each run, Pallas kernels for 20% -> 21%
where the time goes in v3:
time: 183 us; the launch traced here: 179 us
  waiting for transfers between devices  91.5 us (50%)
  Pallas kernels  47.1 us (26%)
  starting transfers between devices  32.9 us (18%)
  matrix products  5.45 us (3%)
    pallas_call x2, Pallas kernels, expert_call(): pl.pallas_call(functools.partial(expert_body, count, own_steps, out_steps...  35.8 us
    ppermute x1, waiting for transfers between devices, on_device(): their_packed = lax.ppermute(packed, 'sp', across)  34.9 us
    ppermute x1, waiting for transfers between devices, on_device(): returned = lax.ppermute(their_sum, 'sp', across).astype(jnp.float32)  31.9 us
    all_to_all x2, waiting for transfers between devices, sent_back(): return exchange(rows.reshape(half, slot_cap, -1)).reshape(local, -1)  20.7 us
    all_to_all x2, starting transfers between devices, sent_back(): return exchange(rows.reshape(half, slot_cap, -1)).reshape(local, -1)  10.3 us
    pallas_call x1, Pallas kernels, front_call(): pl.pallas_call(functools.partial(front_body, taps_count, choose_count, co...  9.09 us
    all_to_all x1, starting transfers between devices, on_device(): own_in = exchange(sendable.reshape(half, slot_cap, model_width))  5.11 us
    all_to_all x1, starting transfers between devices, on_device(): their_in = exchange(their_send)  5.1 us
  transfers between devices with their start and end apart: 16, of which 7 were waited for; matrix products, arithmetic and copies ran while one was open for 2% of the time, Pallas kernels for 21%

profile of v3, /device:TPU:14, one launch (start us, length us, event | category | flops | bytes accessed | tf_op | source)
XLA Modules:
  0.0 179.1 jit_solution(10398576731267943662)
XLA Ops:
  0.5 2.2 %prep_rows.1 = (bf16[64,512]{1,0:T(8,128)(2,1)}, f32[3,512]{1,0:T(4,128)}, f32[8,192]{1,0:T(8,128)}) custom-call(bf16[384,512]{1,0:T(8,128)(2,1)} %refs_0_.3, bf16[384,512]{1,0:T(8,128)(2,1)} %refs_2_.1, f32[1,512]{1,0:T(1,128)} %bitcast.60, f32[1,512]{1,0:T(1,128)} %bitcast.61, f32[1,512]{1,0:T(1,128)} %bitcast.62, s32[2,192]{1,0:T(2,128)} %bitcast.63, ...), custom_call_target="tpu_custom_call" | custom-call | tf_op jit(solution)/shard_map/prep_rows/pallas_call | solution.py:133
  2.8 1.3 collective-permute-start.5
  4.1 3.4 %collective-permute-start.4 = (bf16[64,512]{1,0:T(8,128)(2,1)}, bf16[64,512]{1,0:T(8,128)(2,1)S(1)}, u32[]{:S(2)}, u32[]{:S(2)}) collective-permute-start(bf16[64,512]{1,0:T(8,128)(2,1)} %get-tuple-element.20), channel_id=1, source_target_pairs={{0,2},{2,4},{4,6},{6,8},{8,10},{10,12},{12,14},{14,16},{16,18},{18... | collective-permute-start | bytes 196616 | tf_op jit(solution)/shard_map/ppermute | solution.py:352
  7.6 1.4 collective-permute-done.2.refs_5_
  9.0 1.4 collective-permute-done.4.refs_8_
  10.5 0.7 copy-done
  11.8 9.1 %front_rows.1 = (bf16[192,2048]{1,0:T(8,128)(2,1)}, bf16[192,2048]{1,0:T(8,128)(2,1)}, bf16[384,2048]{1,0:T(8,128)(2,1)}) custom-call(bf16[384,512]{1,0:T(8,128)(2,1)} %refs_0_.3, bf16[384,512]{1,0:T(8,128)(2,1)S(1)} %collective-permute-done.refs_1_, bf16[384,512]{1,0:T(8,128)(2,1)} %refs_2_.1, bf16[384,512]{1,0:T(8,128)(2,1)S(1)} %collective-permute-done.1.refs_3_, ...), custom_call_target="tpu_custom_call" | custom-call | flops 817496064 | bytes 7340032 | tf_op jit(solution)/shard_map/front_rows/pallas_call | solution.py:272
  21.0 5.1 %all-to-all-start = ((bf16[8,48,2048]{2,1,0:T(8,128)(2,1)}), bf16[8,48,2048]{2,1,0:T(8,128)(2,1)S(1)}, u32[]{:S(2)}, u32[]{:S(2)}) async-start(bf16[8,48,2048]{2,1,0:T(8,128)(2,1)} %bitcast.45), calls=%async_computation | async-start | bytes 3145728 | tf_op jit(solution)/shard_map/all_to_all | solution.py:405
  26.6 3.2 %collective-permute-start.6 = (bf16[192,2048]{1,0:T(8,128)(2,1)}, bf16[192,2048]{1,0:T(8,128)(2,1)S(1)}, u32[]{:S(2)}, u32[]{:S(2)}) collective-permute-start(bf16[192,2048]{1,0:T(8,128)(2,1)} %get-tuple-element.25), channel_id=1, source_target_pairs={{0,16},{2,18},{4,20},{6,22},{8,24},{10,26},{12,28},{14,30},{16,0},... | collective-permute-start | bytes 2359304 | tf_op jit(solution)/shard_map/ppermute | solution.py:377
  29.8 34.9 %collective-permute-done.10 = f32[8,192]{1,0:T(8,128)S(1)} collective-permute-done((f32[8,192]{1,0:T(8,128)S(1)}, f32[8,192]{1,0:T(8,128)S(1)}, u32[]{:S(2)}, u32[]{:S(2)}) %collective-permute-start.10) | collective-permute-done | bytes 6176 | tf_op jit(solution)/shard_map/ppermute | solution.py:379
  64.7 1.8 %convolution_convert_fusion = bf16[384,2048]{1,0:T(8,128)(2,1)} fusion(bf16[192,2048]{1,0:T(8,128)(2,1)S(1)} %collective-permute-done.6, s32[192]{0:T(256)S(1)} %bitcast.56, s32[192]{0:T(256)S(1)} %bitcast.55, s32[384]{0:T(512)S(1)} %iota_add_fusion), kind=kOutput, calls=%fused_computation | convolution fusion | flops 302997504 | bytes 2362368 | tf_op jit(solution)/shard_map/dot_general | solution.py:410
  66.5 5.1 %all-to-all-start.1 = ((bf16[8,48,2048]{2,1,0:T(8,128)(2,1)}), bf16[8,48,2048]{2,1,0:T(8,128)(2,1)S(1)}, u32[]{:S(2)}, u32[]{:S(2)}) async-start(bf16[8,48,2048]{2,1,0:T(8,128)(2,1)} %bitcast.44), calls=%async_computation.1 | async-start | bytes 3145728 | tf_op jit(solution)/shard_map/all_to_all | solution.py:412
  71.7 17.9 %expert_rows.2 = bf16[384,2048]{1,0:T(8,128)(2,1)} custom-call(bf16[384,2048]{1,0:T(8,128)(2,1)S(1)} %bitcast.38, bf16[2048,1024]{1,0:T(8,128)(2,1)} %bitcast.65, bf16[2048,1024]{1,0:T(8,128)(2,1)} %collective-permute-done.7.refs_1_, bf16[2048,1024]{1,0:T(8,128)(2,1)} %bitcast.68, bf16[2048,1024]{1,0:T(8,128)(2,1)} %collective-permute-done.8.refs_3_, ...), custom_call_target="tpu_custom_call" | custom-call | flops 9663676416 | bytes 25165824 | tf_op jit(solution)/shard_map/expert_rows/pallas_call | solution.py:65
  89.6 1.1 all-to-all-done.1
  90.7 5.1 %all-to-all-start.2 = ((bf16[8,48,2048]{2,1,0:T(8,128)(2,1)}), bf16[8,48,2048]{2,1,0:T(8,128)(2,1)S(1)}, u32[]{:S(2)}, u32[]{:S(2)}) async-start(bf16[8,48,2048]{2,1,0:T(8,128)(2,1)} %bitcast.47), calls=%async_computation.2 | async-start | bytes 3145728 | tf_op jit(solution)/shard_map/all_to_all | solution.py:394
  95.8 17.9 %expert_rows.3 = bf16[384,2048]{1,0:T(8,128)(2,1)} custom-call(bf16[384,2048]{1,0:T(8,128)(2,1)S(1)} %bitcast.39, bf16[2048,1024]{1,0:T(8,128)(2,1)} %bitcast.66, bf16[2048,1024]{1,0:T(8,128)(2,1)} %collective-permute-done.7.refs_1_, bf16[2048,1024]{1,0:T(8,128)(2,1)} %bitcast.69, bf16[2048,1024]{1,0:T(8,128)(2,1)} %collective-permute-done.8.refs_3_, ...), custom_call_target="tpu_custom_call" | custom-call | flops 9663676416 | bytes 25165824 | tf_op jit(solution)/shard_map/expert_rows/pallas_call | solution.py:65
  113.7 1.6 all-to-all-done.2
  115.2 5.2 %all-to-all-start.3 = ((bf16[8,48,2048]{2,1,0:T(8,128)(2,1)}), bf16[8,48,2048]{2,1,0:T(8,128)(2,1)S(1)}, u32[]{:S(2)}, u32[]{:S(2)}) async-start(bf16[8,48,2048]{2,1,0:T(8,128)(2,1)} %bitcast.46), calls=%async_computation.3 | async-start | bytes 3145728 | tf_op jit(solution)/shard_map/all_to_all | solution.py:394
  120.4 19.1 %all-to-all-done.3 = bf16[8,48,2048]{2,1,0:T(8,128)(2,1)S(1)} async-done(((bf16[8,48,2048]{2,1,0:T(8,128)(2,1)}), bf16[8,48,2048]{2,1,0:T(8,128)(2,1)S(1)}, u32[]{:S(2)}, u32[]{:S(2)}) %all-to-all-start.3) | async-done | bytes 1572896 | tf_op jit(solution)/shard_map/all_to_all | solution.py:394
  140.2 0.7 add_convert_fusion.1
  140.9 3.3 %collective-permute-start.11 = (bf16[192,2048]{1,0:T(8,128)(2,1)S(1)}, bf16[192,2048]{1,0:T(8,128)(2,1)S(1)}, u32[]{:S(2)}, u32[]{:S(2)}) collective-permute-start(bf16[192,2048]{1,0:T(8,128)(2,1)S(1)} %add_convert_fusion.1), channel_id=1, source_target_pairs={{0,16},{2,18},{4,20},{6,22},{8,24},{10,26},{12,28},{14,30},{16,0},... | collective-permute-start | bytes 2359304 | tf_op jit(solution)/shard_map/ppermute | solution.py:421
  144.2 0.7 convert_bitcast_fusion
  145.5 31.9 %collective-permute-done.11 = bf16[192,2048]{1,0:T(8,128)(2,1)S(1)} collective-permute-done((bf16[192,2048]{1,0:T(8,128)(2,1)S(1)}, bf16[192,2048]{1,0:T(8,128)(2,1)S(1)}, u32[]{:S(2)}, u32[]{:S(2)}) %collective-permute-start.11) | collective-permute-done | bytes 786464 | tf_op jit(solution)/shard_map/ppermute | solution.py:421
  177.4 1.7 add_convert_fusion
  (33 shorter events, 3.2 us)
Async XLA Ops:
  0.0 10.4 %collective-permute-start = (bf16[384,512]{1,0:T(8,128)(2,1)}, bf16[384,512]{1,0:T(8,128)(2,1)S(1)}, u32[]{:S(2)}, u32[]{:S(2)}) collective-permute-start(bf16[384,512]{1,0:T(8,128)(2,1)} %refs_0_.3), channel_id=1, source_target_pairs={{0,1},{1,0},{2,3},{3,2},{4,5},{5,4},{6,7},{7,6},{8,9},{9,8},{10,11... | collective-permute-start | bytes 1179656 | tf_op jit(solution)/shard_map/ppermute | solution.py:346
  0.0 10.4 %collective-permute-start.1 = (bf16[384,512]{1,0:T(8,128)(2,1)}, bf16[384,512]{1,0:T(8,128)(2,1)S(1)}, u32[]{:S(2)}, u32[]{:S(2)}) collective-permute-start(bf16[384,512]{1,0:T(8,128)(2,1)} %refs_2_.1), channel_id=1, source_target_pairs={{0,1},{1,0},{2,3},{3,2},{4,5},{5,4},{6,7},{7,6},{8,9},{9,8},{10,11... | collective-permute-start | bytes 1179656 | tf_op jit(solution)/shard_map/ppermute | solution.py:346
  2.7 4.8 %collective-permute-start.3 = (f32[3,512]{1,0:T(4,128)}, f32[3,512]{1,0:T(4,128)S(1)}, u32[]{:S(2)}, u32[]{:S(2)}) collective-permute-start(f32[3,512]{1,0:T(4,128)} %get-tuple-element.19.refs_6_), channel_id=1, source_target_pairs={{0,1},{1,0},{2,3},{3,2},{4,5},{5,4},{6,7},{7,6},{8,9},{9,8},{10,11... | collective-permute-start | bytes 18440 | tf_op jit(solution)/shard_map/ppermute | solution.py:346
  2.8 6.3 %collective-permute-start.5 = (bf16[64,512]{1,0:T(8,128)(2,1)}, bf16[64,512]{1,0:T(8,128)(2,1)S(1)}, u32[]{:S(2)}, u32[]{:S(2)}) collective-permute-start(bf16[64,512]{1,0:T(8,128)(2,1)} %get-tuple-element.20), channel_id=1, source_target_pairs={{1,2},{3,4},{5,6},{7,8},{9,10},{11,12},{13,14},{15,16},{17,18},{19... | collective-permute-start | bytes 196616 | tf_op jit(solution)/shard_map/ppermute | solution.py:352
  4.1 6.4 %collective-permute-start.4 = (bf16[64,512]{1,0:T(8,128)(2,1)}, bf16[64,512]{1,0:T(8,128)(2,1)S(1)}, u32[]{:S(2)}, u32[]{:S(2)}) collective-permute-start(bf16[64,512]{1,0:T(8,128)(2,1)} %get-tuple-element.20), channel_id=1, source_target_pairs={{0,2},{2,4},{4,6},{6,8},{8,10},{10,12},{12,14},{14,16},{16,18},{18... | collective-permute-start | bytes 196616 | tf_op jit(solution)/shard_map/ppermute | solution.py:352
  7.5 1.5 collective-permute-start.2
  10.5 0.7 copy-start
  11.2 0.7 copy-start.1
  21.0 43.8 %all-to-all-start = ((bf16[8,48,2048]{2,1,0:T(8,128)(2,1)}), bf16[8,48,2048]{2,1,0:T(8,128)(2,1)S(1)}, u32[]{:S(2)}, u32[]{:S(2)}) async-start(bf16[8,48,2048]{2,1,0:T(8,128)(2,1)} %bitcast.45), calls=%async_computation | async-start | bytes 3145728 | tf_op jit(solution)/shard_map/all_to_all | solution.py:405
  26.1 45.6 %collective-permute-start.7 = (bf16[2048,1024]{1,0:T(8,128)(2,1)}, bf16[2048,1024]{1,0:T(8,128)(2,1)}, u32[]{:S(2)}, u32[]{:S(2)}) collective-permute-start(bf16[2048,1024]{1,0:T(8,128)(2,1)} %bitcast.64), channel_id=1, source_target_pairs={{0,1},{1,0},{2,3},{3,2},{4,5},{5,4},{6,7},{7,6},{8,9},{9,8},{10,11... | collective-permute-start | bytes 12582920 | tf_op jit(solution)/shard_map/ppermute | solution.py:387
  26.1 45.6 %collective-permute-start.8 = (bf16[2048,1024]{1,0:T(8,128)(2,1)}, bf16[2048,1024]{1,0:T(8,128)(2,1)}, u32[]{:S(2)}, u32[]{:S(2)}) collective-permute-start(bf16[2048,1024]{1,0:T(8,128)(2,1)} %bitcast.67), channel_id=1, source_target_pairs={{0,1},{1,0},{2,3},{3,2},{4,5},{5,4},{6,7},{7,6},{8,9},{9,8},{10,11... | collective-permute-start | bytes 12582920 | tf_op jit(solution)/shard_map/ppermute | solution.py:387
  26.6 45.1 %collective-permute-start.9 = (bf16[1024,2048]{1,0:T(8,128)(2,1)}, bf16[1024,2048]{1,0:T(8,128)(2,1)}, u32[]{:S(2)}, u32[]{:S(2)}) collective-permute-start(bf16[1024,2048]{1,0:T(8,128)(2,1)} %bitcast.70), channel_id=1, source_target_pairs={{0,1},{1,0},{2,3},{3,2},{4,5},{5,4},{6,7},{7,6},{8,9},{9,8},{10,11... | collective-permute-start | bytes 12582920 | tf_op jit(solution)/shard_map/ppermute | solution.py:387
  26.6 38.1 %collective-permute-start.6 = (bf16[192,2048]{1,0:T(8,128)(2,1)}, bf16[192,2048]{1,0:T(8,128)(2,1)S(1)}, u32[]{:S(2)}, u32[]{:S(2)}) collective-permute-start(bf16[192,2048]{1,0:T(8,128)(2,1)} %get-tuple-element.25), channel_id=1, source_target_pairs={{0,16},{2,18},{4,20},{6,22},{8,24},{10,26},{12,28},{14,30},{16,0},... | collective-permute-start | bytes 2359304 | tf_op jit(solution)/shard_map/ppermute | solution.py:377
  29.8 34.9 %collective-permute-start.10 = (f32[8,192]{1,0:T(8,128)S(1)}, f32[8,192]{1,0:T(8,128)S(1)}, u32[]{:S(2)}, u32[]{:S(2)}) collective-permute-start(f32[8,192]{1,0:T(8,128)S(1)} %copy-done), channel_id=1, source_target_pairs={{0,16},{2,18},{4,20},{6,22},{8,24},{10,26},{12,28},{14,30},{16,0},... | collective-permute-start | bytes 18440 | tf_op jit(solution)/shard_map/ppermute | solution.py:379
  66.5 24.1 %all-to-all-start.1 = ((bf16[8,48,2048]{2,1,0:T(8,128)(2,1)}), bf16[8,48,2048]{2,1,0:T(8,128)(2,1)S(1)}, u32[]{:S(2)}, u32[]{:S(2)}) async-start(bf16[8,48,2048]{2,1,0:T(8,128)(2,1)} %bitcast.44), calls=%async_computation.1 | async-start | bytes 3145728 | tf_op jit(solution)/shard_map/all_to_all | solution.py:412
  90.7 24.6 %all-to-all-start.2 = ((bf16[8,48,2048]{2,1,0:T(8,128)(2,1)}), bf16[8,48,2048]{2,1,0:T(8,128)(2,1)S(1)}, u32[]{:S(2)}, u32[]{:S(2)}) async-start(bf16[8,48,2048]{2,1,0:T(8,128)(2,1)} %bitcast.47), calls=%async_computation.2 | async-start | bytes 3145728 | tf_op jit(solution)/shard_map/all_to_all | solution.py:394
  115.2 24.3 %all-to-all-start.3 = ((bf16[8,48,2048]{2,1,0:T(8,128)(2,1)}), bf16[8,48,2048]{2,1,0:T(8,128)(2,1)S(1)}, u32[]{:S(2)}, u32[]{:S(2)}) async-start(bf16[8,48,2048]{2,1,0:T(8,128)(2,1)} %bitcast.46), calls=%async_computation.3 | async-start | bytes 3145728 | tf_op jit(solution)/shard_map/all_to_all | solution.py:394
  140.1 4.1 %copy-start.3 = (f32[192,2]{0,1:T(2,128)S(1)}, f32[192,2]{0,1:T(2,128)}, u32[]{:S(2)}) copy-start(f32[192,2]{0,1:T(2,128)} %param.24) | copy-start | bytes 4612
  140.9 36.6 %collective-permute-start.11 = (bf16[192,2048]{1,0:T(8,128)(2,1)S(1)}, bf16[192,2048]{1,0:T(8,128)(2,1)S(1)}, u32[]{:S(2)}, u32[]{:S(2)}) collective-permute-start(bf16[192,2048]{1,0:T(8,128)(2,1)S(1)} %add_convert_fusion.1), channel_id=1, source_target_pairs={{0,16},{2,18},{4,20},{6,22},{8,24},{10,26},{12,28},{14,30},{16,0},... | collective-permute-start | bytes 2359304 | tf_op jit(solution)/shard_map/ppermute | solution.py:421
  144.9 32.5 %copy-start.2 = (bf16[192,2048]{1,0:T(8,128)(2,1)S(1)}, bf16[192,2048]{1,0:T(8,128)(2,1)}, u32[]{:S(2)}) copy-start(bf16[192,2048]{1,0:T(8,128)(2,1)} %get-tuple-element.22) | copy-start | bytes 2359300

commit v4 on v3

--- a/solution.py
+++ b/solution.py
@@ -296,7 +296,9 @@
         *[near(array) for array in gates[1:]],
         *kernels[:1],
         *[near(array) for array in kernels[1:]],
-        *[near(array) for array in (*vectors, *earlier, slots)],
+        *vectors[:1],
+        *[near(array) for array in (*vectors[1:], *earlier)],
+        slots,
         gain,
         residual_in,
         out_weight,
@@ -419,7 +421,8 @@
     their_out = sent_back(their_parts[0])
     their_sum = weighted(their_out, their_slots.T, their_weights).astype(jnp.bfloat16)
     returned = lax.ppermute(their_sum, "sp", across).astype(jnp.float32)
-    combined = after_f + own_sum + returned
+    settled = lax.optimization_barrier(after_f + own_sum)
+    combined = settled + returned
     return combined.astype(jnp.bfloat16)
 
 

time: 183 us -> 181 us (0.989)
  transfers between devices with their start and end apart: 16 -> 16, of which waited for: 7 -> 7; matrix products, arithmetic and copies ran while one was open for 2% -> 2% of each run, Pallas kernels for 21% -> 22%
where the time goes in v4:
time: 181 us; the launch traced here: 177 us
  waiting for transfers between devices  90.6 us (50%)
  Pallas kernels  47.4 us (26%)
  starting transfers between devices  33.1 us (18%)
  matrix products  4.46 us (2%)
    pallas_call x2, Pallas kernels, expert_call(): pl.pallas_call(functools.partial(expert_body, count, own_steps, out_steps...  36.1 us
    ppermute x1, waiting for transfers between devices, on_device(): their_packed = lax.ppermute(packed, 'sp', across)  34.9 us
    ppermute x1, waiting for transfers between devices, on_device(): returned = lax.ppermute(their_sum, 'sp', across).astype(jnp.float32)  31.4 us
    all_to_all x2, waiting for transfers between devices, sent_back(): return exchange(rows.reshape(half, slot_cap, -1)).reshape(local, -1)  20.5 us
    all_to_all x2, starting transfers between devices, sent_back(): return exchange(rows.reshape(half, slot_cap, -1)).reshape(local, -1)  10.4 us
    pallas_call x1, Pallas kernels, front_call(): pl.pallas_call(functools.partial(front_body, taps_count, choose_count, co...  9.12 us
    all_to_all x1, starting transfers between devices, on_device(): own_in = exchange(sendable.reshape(half, slot_cap, model_width))  5.11 us
    all_to_all x1, starting transfers between devices, on_device(): their_in = exchange(their_send)  5.1 us
  transfers between devices with their start and end apart: 16, of which 7 were waited for; matrix products, arithmetic and copies ran while one was open for 2% of the time, Pallas kernels for 22%

profile of v4, /device:TPU:14, one launch (start us, length us, event | category | flops | bytes accessed | tf_op | source)
XLA Modules:
  0.0 177.3 jit_solution(16486089213526335893)
XLA Ops:
  0.5 2.2 %prep_rows.1 = (bf16[64,512]{1,0:T(8,128)(2,1)}, f32[3,512]{1,0:T(4,128)}, f32[8,192]{1,0:T(8,128)}) custom-call(bf16[384,512]{1,0:T(8,128)(2,1)} %refs_0_.3, bf16[384,512]{1,0:T(8,128)(2,1)} %refs_2_.1, f32[1,512]{1,0:T(1,128)} %bitcast.60, f32[1,512]{1,0:T(1,128)} %bitcast.61, f32[1,512]{1,0:T(1,128)} %bitcast.62, s32[2,192]{1,0:T(2,128)} %bitcast.63, ...), custom_call_target="tpu_custom_call" | custom-call | tf_op jit(solution)/shard_map/prep_rows/pallas_call | solution.py:133
  2.8 1.3 collective-permute-start.5
  4.1 3.4 %collective-permute-start.4 = (bf16[64,512]{1,0:T(8,128)(2,1)}, bf16[64,512]{1,0:T(8,128)(2,1)S(1)}, u32[]{:S(2)}, u32[]{:S(2)}) collective-permute-start(bf16[64,512]{1,0:T(8,128)(2,1)} %get-tuple-element.20), channel_id=1, source_target_pairs={{0,2},{2,4},{4,6},{6,8},{8,10},{10,12},{12,14},{14,16},{16,18},{18... | collective-permute-start | bytes 196616 | tf_op jit(solution)/shard_map/ppermute | solution.py:354
  7.6 1.4 collective-permute-done.2.refs_5_
  9.0 1.4 collective-permute-done.4.refs_8_
  10.5 9.1 %front_rows.1 = (bf16[192,2048]{1,0:T(8,128)(2,1)}, bf16[192,2048]{1,0:T(8,128)(2,1)}, bf16[384,2048]{1,0:T(8,128)(2,1)}) custom-call(bf16[384,512]{1,0:T(8,128)(2,1)} %refs_0_.3, bf16[384,512]{1,0:T(8,128)(2,1)S(1)} %collective-permute-done.refs_1_, bf16[384,512]{1,0:T(8,128)(2,1)} %refs_2_.1, bf16[384,512]{1,0:T(8,128)(2,1)S(1)} %collective-permute-done.1.refs_3_, ...), custom_call_target="tpu_custom_call" | custom-call | flops 817496064 | bytes 7340032 | tf_op jit(solution)/shard_map/front_rows/pallas_call | solution.py:272
  19.6 5.1 %all-to-all-start = ((bf16[8,48,2048]{2,1,0:T(8,128)(2,1)}), bf16[8,48,2048]{2,1,0:T(8,128)(2,1)S(1)}, u32[]{:S(2)}, u32[]{:S(2)}) async-start(bf16[8,48,2048]{2,1,0:T(8,128)(2,1)} %bitcast.45), calls=%async_computation | async-start | bytes 3145728 | tf_op jit(solution)/shard_map/all_to_all | solution.py:407
  25.2 3.2 %collective-permute-start.6 = (bf16[192,2048]{1,0:T(8,128)(2,1)}, bf16[192,2048]{1,0:T(8,128)(2,1)S(1)}, u32[]{:S(2)}, u32[]{:S(2)}) collective-permute-start(bf16[192,2048]{1,0:T(8,128)(2,1)} %get-tuple-element.25), channel_id=1, source_target_pairs={{0,16},{2,18},{4,20},{6,22},{8,24},{10,26},{12,28},{14,30},{16,0},... | collective-permute-start | bytes 2359304 | tf_op jit(solution)/shard_map/ppermute | solution.py:379
  28.5 34.9 %collective-permute-done.10 = f32[8,192]{1,0:T(8,128)S(1)} collective-permute-done((f32[8,192]{1,0:T(8,128)S(1)}, f32[8,192]{1,0:T(8,128)S(1)}, u32[]{:S(2)}, u32[]{:S(2)}) %collective-permute-start.10) | collective-permute-done | bytes 6176 | tf_op jit(solution)/shard_map/ppermute | solution.py:381
  63.4 1.8 %convolution_convert_fusion = bf16[384,2048]{1,0:T(8,128)(2,1)} fusion(bf16[192,2048]{1,0:T(8,128)(2,1)S(1)} %collective-permute-done.6, s32[192]{0:T(256)S(1)} %bitcast.56, s32[192]{0:T(256)S(1)} %bitcast.55, s32[384]{0:T(512)S(1)} %iota_add_fusion), kind=kOutput, calls=%fused_computation | convolution fusion | flops 302997504 | bytes 2362368 | tf_op jit(solution)/shard_map/dot_general | solution.py:412
  65.2 5.1 %all-to-all-start.1 = ((bf16[8,48,2048]{2,1,0:T(8,128)(2,1)}), bf16[8,48,2048]{2,1,0:T(8,128)(2,1)S(1)}, u32[]{:S(2)}, u32[]{:S(2)}) async-start(bf16[8,48,2048]{2,1,0:T(8,128)(2,1)} %bitcast.44), calls=%async_computation.1 | async-start | bytes 3145728 | tf_op jit(solution)/shard_map/all_to_all | solution.py:414
  70.3 18.0 %expert_rows.2 = bf16[384,2048]{1,0:T(8,128)(2,1)} custom-call(bf16[384,2048]{1,0:T(8,128)(2,1)S(1)} %bitcast.38, bf16[2048,1024]{1,0:T(8,128)(2,1)} %bitcast.65, bf16[2048,1024]{1,0:T(8,128)(2,1)} %collective-permute-done.7.refs_1_, bf16[2048,1024]{1,0:T(8,128)(2,1)} %bitcast.68, bf16[2048,1024]{1,0:T(8,128)(2,1)} %collective-permute-done.8.refs_3_, ...), custom_call_target="tpu_custom_call" | custom-call | flops 9663676416 | bytes 25165824 | tf_op jit(solution)/shard_map/expert_rows/pallas_call | solution.py:65
  88.3 1.0 all-to-all-done.1
  89.3 5.1 %all-to-all-start.2 = ((bf16[8,48,2048]{2,1,0:T(8,128)(2,1)}), bf16[8,48,2048]{2,1,0:T(8,128)(2,1)S(1)}, u32[]{:S(2)}, u32[]{:S(2)}) async-start(bf16[8,48,2048]{2,1,0:T(8,128)(2,1)} %bitcast.47), calls=%async_computation.2 | async-start | bytes 3145728 | tf_op jit(solution)/shard_map/all_to_all | solution.py:396
  94.4 18.0 %expert_rows.3 = bf16[384,2048]{1,0:T(8,128)(2,1)} custom-call(bf16[384,2048]{1,0:T(8,128)(2,1)S(1)} %bitcast.39, bf16[2048,1024]{1,0:T(8,128)(2,1)} %bitcast.66, bf16[2048,1024]{1,0:T(8,128)(2,1)} %collective-permute-done.7.refs_1_, bf16[2048,1024]{1,0:T(8,128)(2,1)} %bitcast.69, bf16[2048,1024]{1,0:T(8,128)(2,1)} %collective-permute-done.8.refs_3_, ...), custom_call_target="tpu_custom_call" | custom-call | flops 9663676416 | bytes 25165824 | tf_op jit(solution)/shard_map/expert_rows/pallas_call | solution.py:65
  112.4 1.4 all-to-all-done.2
  113.9 5.3 %all-to-all-start.3 = ((bf16[8,48,2048]{2,1,0:T(8,128)(2,1)}), bf16[8,48,2048]{2,1,0:T(8,128)(2,1)S(1)}, u32[]{:S(2)}, u32[]{:S(2)}) async-start(bf16[8,48,2048]{2,1,0:T(8,128)(2,1)} %bitcast.46), calls=%async_computation.3 | async-start | bytes 3145728 | tf_op jit(solution)/shard_map/all_to_all | solution.py:396
  119.2 19.0 %all-to-all-done.3 = bf16[8,48,2048]{2,1,0:T(8,128)(2,1)S(1)} async-done(((bf16[8,48,2048]{2,1,0:T(8,128)(2,1)}), bf16[8,48,2048]{2,1,0:T(8,128)(2,1)S(1)}, u32[]{:S(2)}, u32[]{:S(2)}) %all-to-all-start.3) | async-done | bytes 1572896 | tf_op jit(solution)/shard_map/all_to_all | solution.py:396
  138.9 0.7 add_convert_fusion.1
  139.6 3.3 %collective-permute-start.11 = (bf16[192,2048]{1,0:T(8,128)(2,1)S(1)}, bf16[192,2048]{1,0:T(8,128)(2,1)S(1)}, u32[]{:S(2)}, u32[]{:S(2)}) collective-permute-start(bf16[192,2048]{1,0:T(8,128)(2,1)S(1)} %add_convert_fusion.1), channel_id=1, source_target_pairs={{0,16},{2,18},{4,20},{6,22},{8,24},{10,26},{12,28},{14,30},{16,0},... | collective-permute-start | bytes 2359304 | tf_op jit(solution)/shard_map/ppermute | solution.py:423
  143.0 0.6 convolution_multiply_fusion.1
  144.1 0.7 convert_add_fusion
  144.8 31.4 %collective-permute-done.11 = bf16[192,2048]{1,0:T(8,128)(2,1)S(1)} collective-permute-done((bf16[192,2048]{1,0:T(8,128)(2,1)S(1)}, bf16[192,2048]{1,0:T(8,128)(2,1)S(1)}, u32[]{:S(2)}, u32[]{:S(2)}) %collective-permute-start.11) | collective-permute-done | bytes 786464 | tf_op jit(solution)/shard_map/ppermute | solution.py:423
  176.2 1.1 add_convert_fusion
  (32 shorter events, 2.4 us)
Async XLA Ops:
  0.0 10.4 %collective-permute-start = (bf16[384,512]{1,0:T(8,128)(2,1)}, bf16[384,512]{1,0:T(8,128)(2,1)S(1)}, u32[]{:S(2)}, u32[]{:S(2)}) collective-permute-start(bf16[384,512]{1,0:T(8,128)(2,1)} %refs_0_.3), channel_id=1, source_target_pairs={{0,1},{1,0},{2,3},{3,2},{4,5},{5,4},{6,7},{7,6},{8,9},{9,8},{10,11... | collective-permute-start | bytes 1179656 | tf_op jit(solution)/shard_map/ppermute | solution.py:348
  0.0 10.4 %collective-permute-start.1 = (bf16[384,512]{1,0:T(8,128)(2,1)}, bf16[384,512]{1,0:T(8,128)(2,1)S(1)}, u32[]{:S(2)}, u32[]{:S(2)}) collective-permute-start(bf16[384,512]{1,0:T(8,128)(2,1)} %refs_2_.1), channel_id=1, source_target_pairs={{0,1},{1,0},{2,3},{3,2},{4,5},{5,4},{6,7},{7,6},{8,9},{9,8},{10,11... | collective-permute-start | bytes 1179656 | tf_op jit(solution)/shard_map/ppermute | solution.py:348
  2.7 4.8 %collective-permute-start.3 = (f32[3,512]{1,0:T(4,128)}, f32[3,512]{1,0:T(4,128)S(1)}, u32[]{:S(2)}, u32[]{:S(2)}) collective-permute-start(f32[3,512]{1,0:T(4,128)} %get-tuple-element.19.refs_6_), channel_id=1, source_target_pairs={{0,1},{1,0},{2,3},{3,2},{4,5},{5,4},{6,7},{7,6},{8,9},{9,8},{10,11... | collective-permute-start | bytes 18440 | tf_op jit(solution)/shard_map/ppermute | solution.py:348
  2.8 6.3 %collective-permute-start.5 = (bf16[64,512]{1,0:T(8,128)(2,1)}, bf16[64,512]{1,0:T(8,128)(2,1)S(1)}, u32[]{:S(2)}, u32[]{:S(2)}) collective-permute-start(bf16[64,512]{1,0:T(8,128)(2,1)} %get-tuple-element.20), channel_id=1, source_target_pairs={{1,2},{3,4},{5,6},{7,8},{9,10},{11,12},{13,14},{15,16},{17,18},{19... | collective-permute-start | bytes 196616 | tf_op jit(solution)/shard_map/ppermute | solution.py:354
  4.1 6.4 %collective-permute-start.4 = (bf16[64,512]{1,0:T(8,128)(2,1)}, bf16[64,512]{1,0:T(8,128)(2,1)S(1)}, u32[]{:S(2)}, u32[]{:S(2)}) collective-permute-start(bf16[64,512]{1,0:T(8,128)(2,1)} %get-tuple-element.20), channel_id=1, source_target_pairs={{0,2},{2,4},{4,6},{6,8},{8,10},{10,12},{12,14},{14,16},{16,18},{18... | collective-permute-start | bytes 196616 | tf_op jit(solution)/shard_map/ppermute | solution.py:354
  7.5 1.5 collective-permute-start.2
  19.6 8.8 %copy-start.1 = (f32[8,192]{1,0:T(8,128)S(1)}, f32[8,192]{1,0:T(8,128)}, u32[]{:S(2)}) copy-start(f32[8,192]{1,0:T(8,128)} %get-tuple-element.24.refs_10_) | copy-start | bytes 18436
  19.6 43.8 %all-to-all-start = ((bf16[8,48,2048]{2,1,0:T(8,128)(2,1)}), bf16[8,48,2048]{2,1,0:T(8,128)(2,1)S(1)}, u32[]{:S(2)}, u32[]{:S(2)}) async-start(bf16[8,48,2048]{2,1,0:T(8,128)(2,1)} %bitcast.45), calls=%async_computation | async-start | bytes 3145728 | tf_op jit(solution)/shard_map/all_to_all | solution.py:407
  24.7 45.6 %collective-permute-start.7 = (bf16[2048,1024]{1,0:T(8,128)(2,1)}, bf16[2048,1024]{1,0:T(8,128)(2,1)}, u32[]{:S(2)}, u32[]{:S(2)}) collective-permute-start(bf16[2048,1024]{1,0:T(8,128)(2,1)} %bitcast.64), channel_id=1, source_target_pairs={{0,1},{1,0},{2,3},{3,2},{4,5},{5,4},{6,7},{7,6},{8,9},{9,8},{10,11... | collective-permute-start | bytes 12582920 | tf_op jit(solution)/shard_map/ppermute | solution.py:389
  24.7 45.6 %collective-permute-start.8 = (bf16[2048,1024]{1,0:T(8,128)(2,1)}, bf16[2048,1024]{1,0:T(8,128)(2,1)}, u32[]{:S(2)}, u32[]{:S(2)}) collective-permute-start(bf16[2048,1024]{1,0:T(8,128)(2,1)} %bitcast.67), channel_id=1, source_target_pairs={{0,1},{1,0},{2,3},{3,2},{4,5},{5,4},{6,7},{7,6},{8,9},{9,8},{10,11... | collective-permute-start | bytes 12582920 | tf_op jit(solution)/shard_map/ppermute | solution.py:389
  25.2 45.1 %collective-permute-start.9 = (bf16[1024,2048]{1,0:T(8,128)(2,1)}, bf16[1024,2048]{1,0:T(8,128)(2,1)}, u32[]{:S(2)}, u32[]{:S(2)}) collective-permute-start(bf16[1024,2048]{1,0:T(8,128)(2,1)} %bitcast.70), channel_id=1, source_target_pairs={{0,1},{1,0},{2,3},{3,2},{4,5},{5,4},{6,7},{7,6},{8,9},{9,8},{10,11... | collective-permute-start | bytes 12582920 | tf_op jit(solution)/shard_map/ppermute | solution.py:389
  25.2 38.1 %collective-permute-start.6 = (bf16[192,2048]{1,0:T(8,128)(2,1)}, bf16[192,2048]{1,0:T(8,128)(2,1)S(1)}, u32[]{:S(2)}, u32[]{:S(2)}) collective-permute-start(bf16[192,2048]{1,0:T(8,128)(2,1)} %get-tuple-element.25), channel_id=1, source_target_pairs={{0,16},{2,18},{4,20},{6,22},{8,24},{10,26},{12,28},{14,30},{16,0},... | collective-permute-start | bytes 2359304 | tf_op jit(solution)/shard_map/ppermute | solution.py:379
  28.4 34.9 %collective-permute-start.10 = (f32[8,192]{1,0:T(8,128)S(1)}, f32[8,192]{1,0:T(8,128)S(1)}, u32[]{:S(2)}, u32[]{:S(2)}) collective-permute-start(f32[8,192]{1,0:T(8,128)S(1)} %copy-done.1), channel_id=1, source_target_pairs={{0,16},{2,18},{4,20},{6,22},{8,24},{10,26},{12,28},{14,30},{16,0},... | collective-permute-start | bytes 18440 | tf_op jit(solution)/shard_map/ppermute | solution.py:381
  65.2 24.1 %all-to-all-start.1 = ((bf16[8,48,2048]{2,1,0:T(8,128)(2,1)}), bf16[8,48,2048]{2,1,0:T(8,128)(2,1)S(1)}, u32[]{:S(2)}, u32[]{:S(2)}) async-start(bf16[8,48,2048]{2,1,0:T(8,128)(2,1)} %bitcast.44), calls=%async_computation.1 | async-start | bytes 3145728 | tf_op jit(solution)/shard_map/all_to_all | solution.py:414
  89.3 24.6 %all-to-all-start.2 = ((bf16[8,48,2048]{2,1,0:T(8,128)(2,1)}), bf16[8,48,2048]{2,1,0:T(8,128)(2,1)S(1)}, u32[]{:S(2)}, u32[]{:S(2)}) async-start(bf16[8,48,2048]{2,1,0:T(8,128)(2,1)} %bitcast.47), calls=%async_computation.2 | async-start | bytes 3145728 | tf_op jit(solution)/shard_map/all_to_all | solution.py:396
  113.9 5.3 %copy-start.2 = (f32[192,2]{0,1:T(2,128)S(1)}, f32[192,2]{0,1:T(2,128)}, u32[]{:S(2)}) copy-start(f32[192,2]{0,1:T(2,128)} %param.24) | copy-start | bytes 4612
  113.9 24.4 %all-to-all-start.3 = ((bf16[8,48,2048]{2,1,0:T(8,128)(2,1)}), bf16[8,48,2048]{2,1,0:T(8,128)(2,1)S(1)}, u32[]{:S(2)}, u32[]{:S(2)}) async-start(bf16[8,48,2048]{2,1,0:T(8,128)(2,1)} %bitcast.46), calls=%async_computation.3 | async-start | bytes 3145728 | tf_op jit(solution)/shard_map/all_to_all | solution.py:396
  139.6 36.6 %collective-permute-start.11 = (bf16[192,2048]{1,0:T(8,128)(2,1)S(1)}, bf16[192,2048]{1,0:T(8,128)(2,1)S(1)}, u32[]{:S(2)}, u32[]{:S(2)}) collective-permute-start(bf16[192,2048]{1,0:T(8,128)(2,1)S(1)} %add_convert_fusion.1), channel_id=1, source_target_pairs={{0,16},{2,18},{4,20},{6,22},{8,24},{10,26},{12,28},{14,30},{16,0},... | collective-permute-start | bytes 2359304 | tf_op jit(solution)/shard_map/ppermute | solution.py:423
  143.0 1.1 copy-start
